TPU v7x, 32 devices: a whole 2x2x4 slice. The times are simulated.
32 devices in a mesh: grp: 2 (over y), ep: 8 (over z, core), tp: 2 (over x).
Axes of the slice: x: 2, y: 2, z: 4, core: 2. Of those that a mesh axis runs over, the one named last changes fastest.
Arguments:
- tokens: bfloat16 [3072, 2048], P(('grp', 'ep')), parts along dimension 0, may hold values from -6 to 6
- norm_gain: float32 [2048], replicated, may hold values from 0.1 to 1.9
- w_gate: bfloat16 [8, 2048, 1024], P('ep', None, 'tp'), may hold values from -0.3125 to 0.3125
- w_up: bfloat16 [8, 2048, 1024], P('ep', None, 'tp'), may hold values from -0.3125 to 0.3125
- w_down: bfloat16 [8, 1024, 2048], P('ep', 'tp'), may hold values from -0.09375 to 0.09375
- expert_ids: int32 [3072, 4], P(('grp', 'ep')), parts along dimension 0, may hold values from 0 to 7, all different within a row; in each aligned block of 192 rows (0 to 191, 192 to 383, ...) at most 128 rows name the same one
- gate_weights: float32 [3072, 4], P(('grp', 'ep')), parts along dimension 0, may hold values from 0.1 to 1
Outputs:
- mixed: bfloat16 [3072, 2048], P(('grp', 'ep'), 'tp'), parts along dimension 0
There are 2 independent parts, one for each index of `grp`. A program takes and returns all parts, laid end to end along the dimension named above; an argument that names none is the same for every part. Nothing has to cross between parts.
Inputs may be any that keep to these rules, and one draw needn't show every extreme that they name: `expert_ids`: each row names 4 different experts; among the rows of one index of ep, no expert is named by more than 128 rows, a bound that some block reaches.
All inputs are finite; a program needn't handle non-finite values.
Results may differ from a plain program's by a relative error of at most 0.012.
Values may be sent and summed in bfloat16 or wider, within the bound.
A program may use at most 64 MiB of HBM per device.

v0:
```python
import functools

import jax
import jax.numpy as jnp
from jax import lax
from jax.experimental import pallas as pl
from jax.experimental.pallas import tpu as pltpu
from jax.sharding import PartitionSpec as P

epsilon = 1e-06
clamp_limit = 7.0
swish_alpha = 1.702


def rms_norm(tokens, norm_gain):
    widened = tokens.astype(jnp.float32)
    scaled = widened * lax.rsqrt(jnp.mean(widened * widened, axis=-1, keepdims=True) + epsilon)
    return (scaled * norm_gain).astype(jnp.bfloat16)


def body(tokens, norm_gain, w_gate, w_up, w_down, expert_ids, gate_weights):
    tok_rows, model_width = tokens.shape
    top_count = expert_ids.shape[1]
    ep_count = lax.axis_size("ep")
    local_experts = w_gate.shape[0]
    experts_all = local_experts * ep_count
    capacity = min(tok_rows, tok_rows * top_count * 4 // (3 * experts_all))
    normed = rms_norm(tokens, norm_gain)
    flat_ids = expert_ids.reshape(-1)
    onehot = (flat_ids[:, None] == jnp.arange(experts_all, dtype=jnp.int32)[None, :]).astype(
        jnp.int32
    )
    before = jnp.cumsum(onehot, axis=0) - onehot
    slot_index = jnp.sum(before * onehot, axis=1)
    dest_row = flat_ids * capacity + slot_index
    owner_tok = jnp.arange(tok_rows * top_count, dtype=jnp.int32) // top_count
    slot_table = (
        jnp.full((experts_all * capacity,), tok_rows, jnp.int32).at[dest_row].set(owner_tok)
    )
    padded = jnp.concatenate([normed, jnp.zeros((1, model_width), jnp.bfloat16)], axis=0)
    send_buffer = padded[slot_table].reshape(experts_all, capacity, model_width)
    received = lax.all_to_all(send_buffer, "ep", split_axis=0, concat_axis=0, tiled=True)
    expert_rows = received.reshape(ep_count, local_experts, capacity, model_width)
    gate_pre = jnp.einsum("sjcd,jdf->sjcf", expert_rows, w_gate, preferred_element_type=jnp.float32)
    up_pre = jnp.einsum("sjcd,jdf->sjcf", expert_rows, w_up, preferred_element_type=jnp.float32)
    gated = jnp.minimum(gate_pre, clamp_limit)
    linear = jnp.clip(up_pre, -clamp_limit, clamp_limit)
    activated = (gated * jax.nn.sigmoid(swish_alpha * gated) * (linear + 1.0)).astype(jnp.bfloat16)
    partial_value = jnp.einsum(
        "sjcf,jfd->sjcd", activated, w_down, preferred_element_type=jnp.float32
    ).astype(jnp.bfloat16)
    summed = (
        lax.psum_scatter(partial_value, "tp", scatter_dimension=3, tiled=True)
        .astype(jnp.float32)
        .astype(jnp.bfloat16)
    )
    returned = lax.all_to_all(summed, "ep", split_axis=0, concat_axis=0, tiled=True)
    returned = returned.reshape(experts_all * capacity, returned.shape[3])
    picked = returned[dest_row].reshape(tok_rows, top_count, returned.shape[1]).astype(jnp.float32)
    return jnp.sum(picked * gate_weights[:, :, None], axis=1).astype(jnp.bfloat16)


MESH = pl.DeviceIdType.MESH
CORES = 2
PIECES = 2
SPLIT = 2
GATE_LANES = 128
COLUMN_TILE = 512
HIDDEN_TILE = 256


def fused_kernel(
    chips,
    tok_ref,
    gain_ref,
    ids_ref,
    gates_ref,
    wg_hbm,
    wu_hbm,
    wd_hbm,
    out_ref,
    rows_all,
    wg,
    wu,
    wd,
    act,
    kept,
    pair_out,
    pair_in,
    side_out,
    side_in,
    part,
    home_out,
    home_in,
    weight_sem,
    own_sem,
    z_send,
    z_recv,
    x_send,
    x_recv,
    c_send,
    c_recv,
    pair_sem,
    side_sem,
    home_send,
    home_recv,
):
    ep, tp = lax.axis_index("ep"), lax.axis_index("tp")
    z, core = lax.div(ep, CORES), lax.rem(ep, CORES)
    rows, width = tok_ref.shape
    half = rows // 2
    piece = half // PIECES
    out_width = width // 2
    experts_all = chips * CORES
    partner = {"ep": z * CORES + 1 - core}
    peer = {"tp": 1 - tp}
    onward = ({"ep": (z + 1) * CORES + core}, {"ep": (z - 1) * CORES + core})
    has_next = (z < chips - 1, z > 0)

    loads = [
        pltpu.make_async_copy(source.at[0], target, weight_sem.at[i])
        for i, (source, target) in enumerate(((wg_hbm, wg), (wu_hbm, wu), (wd_hbm, wd)))
    ]
    for load in loads:
        load.start()

    barrier = pltpu.get_barrier_semaphore()
    for target in (partner, peer):
        pl.semaphore_signal(barrier, inc=1, device_id=target, device_id_type=MESH)
    for side in range(2):

        @pl.when(has_next[side])
        def _(side=side):
            pl.semaphore_signal(barrier, inc=1, device_id=onward[side], device_id_type=MESH)

    widened = tok_ref[...].astype(jnp.float32)
    scaled = widened * lax.rsqrt(jnp.mean(widened * widened, axis=-1, keepdims=True) + epsilon)
    rows_all[z, core, :, :width] = (scaled * gain_ref[...]).astype(jnp.bfloat16)
    code_shape = (GATE_LANES, rows)
    line = lax.broadcasted_iota(jnp.int32, code_shape, 0)
    gate = jnp.zeros(code_shape, jnp.float32)
    for k in range(ids_ref.shape[0]):
        named = lax.rem(line, experts_all) == ids_ref[k : k + 1, :]
        gate = gate + jnp.where(named, gates_ref[k : k + 1, :], 0.0)
    high = gate.astype(jnp.bfloat16).astype(jnp.float32)
    middle = (gate - high).astype(jnp.bfloat16).astype(jnp.float32)
    low = gate - high - middle
    coded = jnp.where(
        line < experts_all,
        high,
        jnp.where(line < 2 * experts_all, middle, jnp.where(line < 3 * experts_all, low, 0.0)),
    ).astype(jnp.bfloat16)
    square = (GATE_LANES, GATE_LANES)
    unit = jnp.where(
        lax.broadcasted_iota(jnp.int32, square, 0) == lax.broadcasted_iota(jnp.int32, square, 1),
        1.0,
        0.0,
    ).astype(jnp.bfloat16)
    rows_all[z, core, :, width:] = lax.dot_general(
        coded, unit, (((0,), (0,)), ((), ())), preferred_element_type=jnp.float32
    ).astype(jnp.bfloat16)

    neighbours = 2 + jnp.where(z > 0, 1, 0) + jnp.where(z < chips - 1, 1, 0)
    pl.semaphore_wait(barrier, neighbours)

    def block_at(side, distance):
        return z - distance if side == 0 else z + distance

    def valid(side, distance):
        return z >= distance if side == 0 else z + distance < chips

    def remote(source, target, send, recv, device):
        return pltpu.make_async_remote_copy(
            src_ref=source,
            dst_ref=target,
            send_sem=send,
            recv_sem=recv,
            device_id=device,
            device_id_type=MESH,
        )

    def rows_of(block, owner, which, q):
        start = pl.multiple_of(which * half + q * piece, 16)
        return rows_all.at[block, owner, pl.ds(start, piece), :]

    def z_copy(side, distance, q):
        ref = rows_of(block_at(side, distance), core, tp, q)
        return remote(
            ref, ref, z_send.at[side, distance, q], z_recv.at[side, distance, q], onward[side]
        )

    def z_arrival(side, distance, q):
        ref = rows_of(block_at(side, distance), core, tp, q)
        return remote(
            ref,
            ref,
            z_send.at[side, distance - 1, q],
            z_recv.at[side, distance - 1, q],
            onward[side],
        )

    def x_copy(side, distance, q, which):
        ref = rows_of(block_at(side, distance), core, which, q)
        return remote(
            ref, ref, x_send.at[side, distance - 1, q], x_recv.at[side, distance - 1, q], peer
        )

    def c_copy(side, distance, q, own_half, owner):
        which = tp if own_half else 1 - tp
        slot = q if own_half else PIECES + q
        ref = rows_of(block_at(side, distance), owner, which, q)
        return remote(
            ref,
            ref,
            c_send.at[side, distance - 1, slot],
            c_recv.at[side, distance - 1, slot],
            partner,
        )

    def own_copy(owner):
        ref = rows_all.at[z, owner]
        return remote(ref, ref, own_sem.at[0], own_sem.at[1], partner)

    for q in range(PIECES):
        for side in range(2):

            @pl.when(has_next[side])
            def _(side=side, q=q):
                z_copy(side, 0, q).start()

    own_copy(core).start()

    def gather_z(distance):
        for q in range(PIECES):
            for side in range(2):

                @pl.when(valid(side, distance))
                def _(side=side, q=q):
                    z_arrival(side, distance, q).wait_recv()

                    if distance < chips - 1:

                        @pl.when(has_next[side])
                        def _():
                            z_copy(side, distance, q).start()

                    x_copy(side, distance, q, tp).start()
                    c_copy(side, distance, q, True, core).start()

    def gather_x(distance):
        for q in range(PIECES):
            for side in range(2):

                @pl.when(valid(side, distance))
                def _(side=side, q=q):
                    x_copy(side, distance, q, 1 - tp).wait_recv()
                    c_copy(side, distance, q, False, core).start()

    def span_of(q):
        return pl.ds(q * (rows // SPLIT), rows // SPLIT)

    def pair_copy(block, q):
        return remote(
            pair_out.at[block, span_of(q)],
            pair_in.at[block, span_of(q)],
            pair_sem.at[0, block, q],
            pair_sem.at[1, block, q],
            partner,
        )

    def side_copy(block, q):
        return remote(
            side_out.at[block, span_of(q)],
            side_in.at[block, span_of(q)],
            side_sem.at[0, block, q],
            side_sem.at[1, block, q],
            peer,
        )

    def home_copy(source, dest, q):
        return remote(
            home_out.at[dest, span_of(q)],
            home_in.at[source, span_of(q)],
            home_send.at[dest, q],
            home_recv.at[source, q],
            {"ep": dest * CORES + core},
        )

    def expert(block):
        held = jnp.concatenate(
            [rows_all[block, core, :, :width], rows_all[block, 1 - core, :, :width]], axis=0
        )
        code = jnp.concatenate(
            [rows_all[block, core, :, width:], rows_all[block, 1 - core, :, width:]], axis=0
        ).astype(jnp.float32)
        code_lane = lax.broadcasted_iota(jnp.int32, code.shape, 1)
        weight = jnp.sum(
            jnp.where(lax.rem(code_lane, experts_all) == ep, code, 0.0), axis=1, keepdims=True
        )
        for start in range(0, wg.shape[1], HIDDEN_TILE):
            columns = slice(start, start + HIDDEN_TILE)
            gate_pre = jnp.dot(held, wg[:, columns], preferred_element_type=jnp.float32)
            up_pre = jnp.dot(held, wu[:, columns], preferred_element_type=jnp.float32)
            gated = jnp.minimum(gate_pre, clamp_limit)
            linear = jnp.clip(up_pre, -clamp_limit, clamp_limit)
            act[:, columns] = (gated * jax.nn.sigmoid(swish_alpha * gated) * (linear + 1.0)).astype(
                jnp.bfloat16
            )
        for start in range(0, width, COLUMN_TILE):
            columns = slice(start, start + COLUMN_TILE)
            partial_value = (
                jnp.dot(act[...], wd[:, columns], preferred_element_type=jnp.float32) * weight
            )
            kept[block, :, columns] = partial_value[:rows]
            pair_out[block, :, columns] = partial_value[rows:].astype(jnp.bfloat16)
        for q in range(SPLIT):
            pair_copy(block, q).start()

    def experts_at(distance):
        def one(side, carry):
            block = z + distance * (2 * side - 1)

            @pl.when((block >= 0) & (block < chips))
            def _():
                for q in range(PIECES):
                    for own_half in (True, False):
                        which = tp if own_half else 1 - tp
                        slot = q if own_half else PIECES + q
                        ref = rows_of(block, 1 - core, which, q)
                        remote(
                            ref,
                            ref,
                            c_send.at[side, distance - 1, slot],
                            c_recv.at[side, distance - 1, slot],
                            partner,
                        ).wait_recv()
                expert(block)

            return carry

        lax.fori_loop(0, 2, one, 0)

    def each(distance, action):
        if distance == 0:
            action(z)
            return
        for side in range(2):

            @pl.when(valid(side, distance))
            def _(side=side):
                action(block_at(side, distance))

    theirs = pl.ds(pl.multiple_of((1 - tp) * out_width, 128), out_width)
    mine = pl.ds(pl.multiple_of(tp * out_width, 128), out_width)

    def pair_sum(block):
        for q in range(SPLIT):
            pair_copy(block, q).wait_recv()
            span = span_of(q)
            side_out[block, span] = (
                kept[block, span, theirs] + pair_in[block, span, theirs].astype(jnp.float32)
            ).astype(jnp.bfloat16)
            side_copy(block, q).start()
        for q in range(SPLIT):
            span = span_of(q)
            part[block, span] = kept[block, span, mine] + pair_in[block, span, mine].astype(
                jnp.float32
            )

    def side_sum(block):
        for q in range(SPLIT):
            side_copy(block, q).wait_recv()
            span = span_of(q)
            home_out[block, span] = (
                part[block, span] + side_in[block, span].astype(jnp.float32)
            ).astype(jnp.bfloat16)
            home_copy(z, block, q).start()

    def own_side_sum():
        for q in range(SPLIT):
            side_copy(z, q).wait_recv()
            span = span_of(q)
            part[z, span] = part[z, span] + side_in[z, span].astype(jnp.float32)

    def take_in(source):
        for q in range(SPLIT):
            home_copy(source, z, q).wait_recv()
            span = span_of(q)
            part[z, span] = part[z, span] + home_in[source, span].astype(jnp.float32)

    own_copy(1 - core).wait_recv()
    for load in loads:
        load.wait()
    last = chips - 1
    expert(z)
    for turn in range(1, min(2, last) + 1):
        gather_z(turn)
    for turn in range(1, last + 1):
        gather_x(turn)
        experts_at(turn)
        if turn + 2 <= last:
            gather_z(turn + 2)
        each(turn, pair_sum)
    for distance in range(1, last):
        each(distance, side_sum)
    pair_sum(z)
    each(last, side_sum)
    own_side_sum()
    for distance in range(1, chips):
        each(distance, take_in)
    out_ref[...] = part[z].astype(jnp.bfloat16)

    own_copy(core).wait_send()
    for q in range(PIECES):
        for side in range(2):
            for distance in range(chips):
                if distance < last:

                    @pl.when(valid(side, distance) & has_next[side])
                    def _(side=side, distance=distance, q=q):
                        z_copy(side, distance, q).wait_send()

                if distance > 0:

                    @pl.when(valid(side, distance))
                    def _(side=side, distance=distance, q=q):
                        x_copy(side, distance, q, tp).wait_send()
                        c_copy(side, distance, q, True, core).wait_send()
                        c_copy(side, distance, q, False, core).wait_send()

    for q in range(SPLIT):
        for block in range(chips):
            pair_copy(block, q).wait_send()
            side_copy(block, q).wait_send()
        for distance in range(1, chips):
            each(distance, lambda block, q=q: home_copy(z, block, q).wait_send())


def fused(tokens, norm_gain, w_gate, w_up, w_down, expert_ids, gate_weights):
    rows, width = tokens.shape
    chips = lax.axis_size("ep") // CORES
    hidden = w_gate.shape[2]
    out_width = width // 2
    last = chips - 1
    vmem = pl.BlockSpec(memory_space=pltpu.VMEM)
    anywhere = pl.BlockSpec(memory_space=pl.ANY)
    dma = pltpu.SemaphoreType.DMA
    return pl.pallas_call(
        functools.partial(fused_kernel, chips),
        out_shape=jax.ShapeDtypeStruct((rows, out_width), jnp.bfloat16),
        in_specs=[vmem] * 4 + [anywhere] * 3,
        out_specs=vmem,
        scratch_shapes=[
            pltpu.VMEM((chips, CORES, rows, width + GATE_LANES), jnp.bfloat16),
            pltpu.VMEM((width, hidden), jnp.bfloat16),
            pltpu.VMEM((width, hidden), jnp.bfloat16),
            pltpu.VMEM((hidden, width), jnp.bfloat16),
            pltpu.VMEM((CORES * rows, hidden), jnp.bfloat16),
            pltpu.VMEM((chips, rows, width), jnp.float32),
            pltpu.VMEM((chips, rows, width), jnp.bfloat16),
            pltpu.VMEM((chips, rows, width), jnp.bfloat16),
            pltpu.VMEM((chips, rows, out_width), jnp.bfloat16),
            pltpu.VMEM((chips, rows, out_width), jnp.bfloat16),
            pltpu.VMEM((chips, rows, out_width), jnp.float32),
            pltpu.VMEM((chips, rows, out_width), jnp.bfloat16),
            pltpu.VMEM((chips, rows, out_width), jnp.bfloat16),
            dma((3,)),
            dma((2,)),
            dma((2, last, PIECES)),
            dma((2, last, PIECES)),
            dma((2, last, PIECES)),
            dma((2, last, PIECES)),
            dma((2, last, 2 * PIECES)),
            dma((2, last, 2 * PIECES)),
            dma((2, chips, SPLIT)),
            dma((2, chips, SPLIT)),
            dma((chips, SPLIT)),
            dma((chips, SPLIT)),
        ],
        compiler_params=pltpu.CompilerParams(collective_id=0, has_side_effects=True),
    )(tokens, norm_gain[None, :], expert_ids.T, gate_weights.T, w_gate, w_up, w_down)


def step(mesh, *arrays):
    tokens, norm_gain, w_gate, w_up, w_down, expert_ids, gate_weights = arrays
    ep_count, tp_count = mesh.shape["ep"], mesh.shape["tp"]
    rows, top_count = expert_ids.shape
    experts_all = ep_count * w_gate.shape[0]
    capacity = min(rows, rows * top_count * 4 // (3 * experts_all))
    dense = (
        w_gate.shape[0] == 1
        and tp_count == 2
        and ep_count % CORES == 0
        and ep_count > CORES
        and rows <= 2 * capacity
        and 3 * experts_all <= GATE_LANES
        and rows % (32 * PIECES) == 0
    )
    return fused(*arrays) if dense else body(*arrays)


def solution(mesh):
    placed = (
        P(("grp", "ep"), None),
        P(),
        P("ep", None, "tp"),
        P("ep", None, "tp"),
        P("ep", "tp", None),
        P(("grp", "ep"), None),
        P(("grp", "ep"), None),
    )
    return jax.shard_map(
        functools.partial(step, mesh), mesh=mesh, in_specs=placed, out_specs=P(("grp", "ep"), "tp"), check_vma=False
    )
```

profile of v0, /device:TPU:0, one launch (start us, length us, event | category | flops | bytes accessed | tf_op | source)
XLA Modules:
  0.0 88.0 jit_solution(5352803337893128407)
XLA Ops:
  0.0 86.2 %shard_map.73 = bf16[192,1024]{1,0:T(8,128)(2,1)} custom-call(bf16[192,2048]{1,0:T(8,128)(2,1)} %tok_ref.1, f32[1,2048]{1,0:T(1,128)} %bitcast.3, s32[4,192]{1,0:T(4,128)} %bitcast.4, f32[4,192]{1,0:T(4,128)} %bitcast.5, bf16[1,2048,512]{2,1,0:T(8,128)(2,1)} %wg_hbm.1, bf16[1,2048,512]{2,1,0:T(8,128)(2,1)} %wu_hbm.1, bf16[1,512,2048]{2,1,0:T(8,128)(2,1)} %wd_hbm.1), custom_call_target="tpu_custom_call" | custom-call | tf_op jit(solution)/shard_map/pallas_call | solution.py:448
  86.2 1.8 %copy.9 = bf16[192,1024]{1,0:T(8,128)(2,1)} copy(bf16[192,1024]{1,0:T(8,128)(2,1)} %shard_map.73) | data formatting | bytes 786432
where the time goes:
time: 88.4 us; the launch traced here: 88 us
  Pallas kernels  86.2 us (98%)
  local copies, waits for them, and re-layouts  1.77 us (2%)
    pallas_call x1, Pallas kernels, fused(): pl.pallas_call(functools.partial(fused_kernel, chips), out_shape=jax.Shap...  86.2 us

commit v1 on v0

v1 whole, which is shorter than its diff:
```python
import functools

import jax
import jax.numpy as jnp
from jax import lax
from jax.experimental import pallas as pl
from jax.experimental.pallas import tpu as pltpu
from jax.sharding import PartitionSpec as P

epsilon = 1e-06
clamp_limit = 7.0
swish_alpha = 1.702


def rms_norm(tokens, norm_gain):
    widened = tokens.astype(jnp.float32)
    scaled = widened * lax.rsqrt(jnp.mean(widened * widened, axis=-1, keepdims=True) + epsilon)
    return (scaled * norm_gain).astype(jnp.bfloat16)


def body(tokens, norm_gain, w_gate, w_up, w_down, expert_ids, gate_weights):
    tok_rows, model_width = tokens.shape
    top_count = expert_ids.shape[1]
    ep_count = lax.axis_size("ep")
    local_experts = w_gate.shape[0]
    experts_all = local_experts * ep_count
    capacity = min(tok_rows, tok_rows * top_count * 4 // (3 * experts_all))
    normed = rms_norm(tokens, norm_gain)
    flat_ids = expert_ids.reshape(-1)
    onehot = (flat_ids[:, None] == jnp.arange(experts_all, dtype=jnp.int32)[None, :]).astype(
        jnp.int32
    )
    before = jnp.cumsum(onehot, axis=0) - onehot
    slot_index = jnp.sum(before * onehot, axis=1)
    dest_row = flat_ids * capacity + slot_index
    owner_tok = jnp.arange(tok_rows * top_count, dtype=jnp.int32) // top_count
    slot_table = (
        jnp.full((experts_all * capacity,), tok_rows, jnp.int32).at[dest_row].set(owner_tok)
    )
    padded = jnp.concatenate([normed, jnp.zeros((1, model_width), jnp.bfloat16)], axis=0)
    send_buffer = padded[slot_table].reshape(experts_all, capacity, model_width)
    received = lax.all_to_all(send_buffer, "ep", split_axis=0, concat_axis=0, tiled=True)
    expert_rows = received.reshape(ep_count, local_experts, capacity, model_width)
    gate_pre = jnp.einsum("sjcd,jdf->sjcf", expert_rows, w_gate, preferred_element_type=jnp.float32)
    up_pre = jnp.einsum("sjcd,jdf->sjcf", expert_rows, w_up, preferred_element_type=jnp.float32)
    gated = jnp.minimum(gate_pre, clamp_limit)
    linear = jnp.clip(up_pre, -clamp_limit, clamp_limit)
    activated = (gated * jax.nn.sigmoid(swish_alpha * gated) * (linear + 1.0)).astype(jnp.bfloat16)
    partial_value = jnp.einsum(
        "sjcf,jfd->sjcd", activated, w_down, preferred_element_type=jnp.float32
    ).astype(jnp.bfloat16)
    summed = (
        lax.psum_scatter(partial_value, "tp", scatter_dimension=3, tiled=True)
        .astype(jnp.float32)
        .astype(jnp.bfloat16)
    )
    returned = lax.all_to_all(summed, "ep", split_axis=0, concat_axis=0, tiled=True)
    returned = returned.reshape(experts_all * capacity, returned.shape[3])
    picked = returned[dest_row].reshape(tok_rows, top_count, returned.shape[1]).astype(jnp.float32)
    return jnp.sum(picked * gate_weights[:, :, None], axis=1).astype(jnp.bfloat16)


MESH = pl.DeviceIdType.MESH
CORES = 2
PIECES = 3
SPLIT = 3
HIDDEN_TILE = 256
COLUMN_TILE = 512


def fused_kernel(
    chips,
    tok_ref,
    gain_ref,
    ids_ref,
    gates_ref,
    wg_hbm,
    wu_hbm,
    wd_hbm,
    out_ref,
    rows_all,
    codes,
    wg,
    wu,
    wd,
    act,
    kept,
    part,
    merge_out,
    merge_in,
    side_out,
    side_in,
    far_out,
    far_in,
    agg_in,
    weight_sem,
    pair_sem,
    code_send,
    code_recv,
    z_send,
    z_recv,
    x_send,
    x_recv,
    merge_sem,
    side_sem,
    far_send,
    far_recv,
):
    ep, tp = lax.axis_index("ep"), lax.axis_index("tp")
    z, core = lax.div(ep, CORES), lax.rem(ep, CORES)
    rows, width = tok_ref.shape
    half = rows // 2
    piece = half // PIECES
    out_width = width // 2
    hidden = wg.shape[2]
    last = chips - 1
    partner = {"ep": z * CORES + 1 - core}
    peer = {"tp": 1 - tp}
    onward = ({"ep": (z + 1) * CORES + core}, {"ep": (z - 1) * CORES + core})
    has_next = (z < last, z > 0)

    sources = (wg_hbm.at[0], wu_hbm.at[0], wd_hbm.at[0])
    loads = [
        pltpu.make_async_copy(source, target, weight_sem.at[i])
        for i, (source, target) in enumerate(
            zip(sources, (wg.at[0], wu.at[0], wd.at[pl.ds(0, hidden)]))
        )
    ]
    for load in loads:
        load.start()

    barrier = pltpu.get_barrier_semaphore()
    for target in (partner, peer):
        pl.semaphore_signal(barrier, inc=1, device_id=target, device_id_type=MESH)
    for side in range(2):

        @pl.when(has_next[side])
        def _(side=side):
            pl.semaphore_signal(barrier, inc=1, device_id=onward[side], device_id_type=MESH)

    def block_at(side, distance):
        return z - distance if side == 0 else z + distance

    def valid(side, distance):
        return z >= distance if side == 0 else z + distance < chips

    def remote(source, target, send, recv, device):
        return pltpu.make_async_remote_copy(
            src_ref=source,
            dst_ref=target,
            send_sem=send,
            recv_sem=recv,
            device_id=device,
            device_id_type=MESH,
        )

    def chip_of(block):
        return {"ep": block * CORES + core}

    gives = [
        remote(source, target, pair_sem.at[0, i], pair_sem.at[1, i], partner)
        for i, (source, target) in enumerate(
            zip(sources, (wg.at[1], wu.at[1], wd.at[pl.ds(hidden, hidden)]))
        )
    ]

    def normed(start):
        span = pl.ds(pl.multiple_of(start, 16), half)
        widened = tok_ref[span].astype(jnp.float32)
        scaled = widened * lax.rsqrt(jnp.mean(widened * widened, axis=-1, keepdims=True) + epsilon)
        rows_all[z, span] = (scaled * gain_ref[...]).astype(jnp.bfloat16)

    normed(tp * half)
    line = lax.broadcasted_iota(jnp.int32, codes.shape[1:], 0)
    gate = jnp.zeros(codes.shape[1:], jnp.float32)
    for k in range(ids_ref.shape[0]):
        gate = gate + jnp.where(line == ids_ref[k : k + 1, :], gates_ref[k : k + 1, :], 0.0)
    codes[z] = gate

    neighbours = 2 + jnp.where(z > 0, 1, 0) + jnp.where(z < last, 1, 0)
    pl.semaphore_wait(barrier, neighbours)

    def rows_of(block, which, q):
        start = pl.multiple_of(which * half + q * piece, 16)
        return rows_all.at[block, pl.ds(start, piece), :]

    def z_copy(side, distance, q):
        ref = rows_of(block_at(side, distance), tp, q)
        return remote(
            ref, ref, z_send.at[side, distance, q], z_recv.at[side, distance, q], onward[side]
        )

    def z_arrival(side, distance, q):
        ref = rows_of(block_at(side, distance), tp, q)
        return remote(
            ref,
            ref,
            z_send.at[side, distance - 1, q],
            z_recv.at[side, distance - 1, q],
            onward[side],
        )

    def code_copy(side, distance, hop):
        ref = codes.at[block_at(side, distance)]
        return remote(ref, ref, code_send.at[side, hop], code_recv.at[side, hop], onward[side])

    def x_copy(side, distance, q, which):
        ref = rows_of(block_at(side, distance), which, q)
        return remote(
            ref, ref, x_send.at[side, distance - 1, q], x_recv.at[side, distance - 1, q], peer
        )

    for q in range(PIECES):
        for side in range(2):

            @pl.when(has_next[side])
            def _(side=side, q=q):
                z_copy(side, 0, q).start()
                if q == 0:
                    code_copy(side, 0, 0).start()

    for give in gives:
        give.start()
    normed((1 - tp) * half)

    def gather_z(distance, pieces):
        for q in pieces:
            for side in range(2):

                @pl.when(valid(side, distance))
                def _(side=side, q=q):
                    z_arrival(side, distance, q).wait_recv()
                    if q == 0:
                        code_copy(side, distance, distance - 1).wait_recv()
                    if distance < last:

                        @pl.when(has_next[side])
                        def _():
                            z_copy(side, distance, q).start()
                            if q == 0:
                                code_copy(side, distance, distance).start()

                    x_copy(side, distance, q, tp).start()

    def gather_x(distance):
        for q in range(PIECES):
            for side in range(2):

                @pl.when(valid(side, distance))
                def _(side=side, q=q):
                    x_copy(side, distance, q, 1 - tp).wait_recv()

    theirs = pl.multiple_of((1 - tp) * out_width, 128)
    mine = pl.multiple_of(tp * out_width, 128)

    def span_of(q):
        return pl.ds(q * (rows // SPLIT), rows // SPLIT)

    def activate(block, slot):
        turned = jnp.transpose(codes[block])
        lane = lax.broadcasted_iota(jnp.int32, turned.shape, 1)
        owner = ep if slot == 0 else z * CORES + 1 - core
        weight = jnp.sum(jnp.where(lane == owner, turned, 0.0), axis=1, keepdims=True)[:rows]
        held = rows_all[block]
        for start in range(0, hidden, HIDDEN_TILE):
            columns = slice(start, start + HIDDEN_TILE)
            gate_pre = jnp.dot(held, wg[slot, :, columns], preferred_element_type=jnp.float32)
            up_pre = jnp.dot(held, wu[slot, :, columns], preferred_element_type=jnp.float32)
            gated = jnp.minimum(gate_pre, clamp_limit)
            linear = jnp.clip(up_pre, -clamp_limit, clamp_limit)
            value = gated * jax.nn.sigmoid(swish_alpha * gated) * (linear + 1.0) * weight
            act[:, slot * hidden + start : slot * hidden + start + HIDDEN_TILE] = value.astype(
                jnp.bfloat16
            )

    def project(start):
        return jnp.dot(
            act[...], wd[:, pl.ds(start, COLUMN_TILE)], preferred_element_type=jnp.float32
        )

    def merge_copy(side, other, q, block):
        return remote(
            merge_out.at[side, span_of(q)],
            merge_in.at[other, span_of(q)],
            merge_sem.at[0, side, q],
            merge_sem.at[1, other, q],
            chip_of(block),
        )

    def side_copy(block, q):
        return remote(
            side_out.at[block, span_of(q)],
            side_in.at[block, span_of(q)],
            side_sem.at[0, block, q],
            side_sem.at[1, block, q],
            peer,
        )

    def far_copy(side, distance, q):
        dest = block_at(side, distance)
        sender = far_send.at[side, distance - 2, q]
        if distance == 2:
            target, receiver = far_in.at[1 - side, span_of(q)], far_recv.at[1 - side, 0, q]
            device = chip_of(dest)
        else:
            target = agg_in.at[side, distance - 3, span_of(q)]
            receiver = far_recv.at[side, distance - 2, q]
            device = onward[1 - side]
        return remote(far_out.at[dest, span_of(q)], target, sender, receiver, device)

    def far_arrival(side, q):
        return remote(
            far_in.at[side, span_of(q)],
            far_in.at[side, span_of(q)],
            far_send.at[side, 0, q],
            far_recv.at[side, 0, q],
            peer,
        )

    def agg_arrival(side, distance, q):
        ref = agg_in.at[side, distance - 2, span_of(q)]
        return remote(
            ref, ref, far_send.at[side, 0, q], far_recv.at[side, distance - 1, q], peer
        )

    def experts_at(distance):
        def one(side, carry):
            block = z + distance * (2 * side - 1)

            @pl.when((block >= 0) & (block < chips))
            def _():
                activate(block, 0)
                activate(block, 1)
                if distance == 1:
                    for start in range(0, width, COLUMN_TILE):
                        merge_out[side, :, start : start + COLUMN_TILE] = project(start).astype(
                            jnp.bfloat16
                        )
                    for q in range(SPLIT):
                        merge_copy(side, 1 - side, q, block).start()
                else:
                    for start in range(0, out_width, COLUMN_TILE):
                        side_out[block, :, start : start + COLUMN_TILE] = project(
                            pl.multiple_of(theirs + start, 128)
                        ).astype(jnp.bfloat16)
                    for q in range(SPLIT):
                        side_copy(block, q).start()
                    for start in range(0, out_width, COLUMN_TILE):
                        part[block, :, start : start + COLUMN_TILE] = project(
                            pl.multiple_of(mine + start, 128)
                        )

            return carry

        lax.fori_loop(0, 2, one, 0)

    def far_sum(side, distance, more):
        block = block_at(side, distance)
        for q in range(SPLIT):
            span = span_of(q)
            side_copy(block, q).wait_recv()
            total = part[block, span] + side_in[block, span].astype(jnp.float32)
            if more:
                agg_arrival(side, distance, q).wait_recv()
                total = total + agg_in[side, distance - 2, span].astype(jnp.float32)
            far_out[block, span] = total.astype(jnp.bfloat16)
            far_copy(side, distance, q).start()

    def far_sums(distance, more):
        for side in range(2):
            through = has_next[side]

            @pl.when(valid(side, distance) & (through if more else jnp.logical_not(through)))
            def _(side=side):
                far_sum(side, distance, more)

    def own_exchange():
        for q in range(SPLIT):
            span = span_of(q)
            for side in range(2):

                @pl.when(valid(side, 1))
                def _(side=side, q=q):
                    merge_copy(1 - side, side, q, block_at(side, 1)).wait_recv()
                    kept[span] = kept[span] + merge_in[side, span].astype(jnp.float32)

            side_out[z, span] = kept[span, pl.ds(theirs, out_width)].astype(jnp.bfloat16)
            side_copy(z, q).start()

    def finish():
        for q in range(SPLIT):
            span = span_of(q)
            side_copy(z, q).wait_recv()
            part[z, span] = kept[span, pl.ds(mine, out_width)] + side_in[z, span].astype(
                jnp.float32
            )
            if chips > 2:
                for side in range(2):

                    @pl.when(valid(side, 2))
                    def _(side=side, q=q):
                        far_arrival(side, q).wait_recv()
                        part[z, span] = part[z, span] + far_in[side, span].astype(jnp.float32)

            out_ref[span] = part[z, span].astype(jnp.bfloat16)

    for load in loads:
        load.wait()
    activate(z, 0)
    gather_z(1, range(PIECES - 1))
    for give in gives[:2]:
        give.wait_recv()
    activate(z, 1)
    gather_z(1, range(PIECES - 1, PIECES))
    gives[2].wait_recv()
    for start in range(0, width, COLUMN_TILE):
        kept[:, start : start + COLUMN_TILE] = project(start)
    if last >= 2:
        gather_z(2, range(PIECES))
    for turn in range(1, last + 1):
        gather_x(turn)
        experts_at(turn)
        if turn + 2 <= last:
            gather_z(turn + 2, range(PIECES))
    for distance in range(2, last):
        far_sums(distance, False)
    own_exchange()
    if last >= 2:
        far_sums(last, False)
    for distance in range(last - 1, 1, -1):
        far_sums(distance, True)
    finish()

    for give in gives:
        give.wait_send()
    for q in range(PIECES):
        for side in range(2):
            for distance in range(chips):
                if distance < last:

                    @pl.when(valid(side, distance) & has_next[side])
                    def _(side=side, distance=distance, q=q):
                        z_copy(side, distance, q).wait_send()
                        if q == 0:
                            code_copy(side, distance, distance).wait_send()

                if distance > 0:

                    @pl.when(valid(side, distance))
                    def _(side=side, distance=distance, q=q):
                        x_copy(side, distance, q, tp).wait_send()

    for q in range(SPLIT):
        side_copy(z, q).wait_send()
        for side in range(2):
            for distance in range(1, chips):

                @pl.when(valid(side, distance))
                def _(side=side, distance=distance, q=q):
                    if distance == 1:
                        merge_copy(side, 1 - side, q, block_at(side, 1)).wait_send()
                    else:
                        side_copy(block_at(side, distance), q).wait_send()
                        far_copy(side, distance, q).wait_send()


def fused(tokens, norm_gain, w_gate, w_up, w_down, expert_ids, gate_weights):
    rows, width = tokens.shape
    chips = lax.axis_size("ep") // CORES
    experts_all = chips * CORES
    hidden = w_gate.shape[2]
    out_width = width // 2
    last = chips - 1
    hops = max(last - 1, 1)
    lanes = -rows % 128
    vmem = pl.BlockSpec(memory_space=pltpu.VMEM)
    anywhere = pl.BlockSpec(memory_space=pl.ANY)
    dma = pltpu.SemaphoreType.DMA
    ids = jnp.pad(expert_ids.T, ((0, 0), (0, lanes)), constant_values=-1)
    gates = jnp.pad(gate_weights.T, ((0, 0), (0, lanes)))
    return pl.pallas_call(
        functools.partial(fused_kernel, chips),
        out_shape=jax.ShapeDtypeStruct((rows, out_width), jnp.bfloat16),
        in_specs=[vmem] * 4 + [anywhere] * 3,
        out_specs=vmem,
        scratch_shapes=[
            pltpu.VMEM((chips, rows, width), jnp.bfloat16),
            pltpu.VMEM((chips, experts_all + -experts_all % 8, rows + lanes), jnp.float32),
            pltpu.VMEM((CORES, width, hidden), jnp.bfloat16),
            pltpu.VMEM((CORES, width, hidden), jnp.bfloat16),
            pltpu.VMEM((CORES * hidden, width), jnp.bfloat16),
            pltpu.VMEM((rows, CORES * hidden), jnp.bfloat16),
            pltpu.VMEM((rows, width), jnp.float32),
            pltpu.VMEM((chips, rows, out_width), jnp.float32),
            pltpu.VMEM((2, rows, width), jnp.bfloat16),
            pltpu.VMEM((2, rows, width), jnp.bfloat16),
            pltpu.VMEM((chips, rows, out_width), jnp.bfloat16),
            pltpu.VMEM((chips, rows, out_width), jnp.bfloat16),
            pltpu.VMEM((chips, rows, out_width), jnp.bfloat16),
            pltpu.VMEM((2, rows, out_width), jnp.bfloat16),
            pltpu.VMEM((2, hops, rows, out_width), jnp.bfloat16),
            dma((3,)),
            dma((2, 3)),
            dma((2, last)),
            dma((2, last)),
            dma((2, last, PIECES)),
            dma((2, last, PIECES)),
            dma((2, last, PIECES)),
            dma((2, last, PIECES)),
            dma((2, 2, SPLIT)),
            dma((2, chips, SPLIT)),
            dma((2, hops, SPLIT)),
            dma((2, hops + 1, SPLIT)),
        ],
        compiler_params=pltpu.CompilerParams(collective_id=0, has_side_effects=True),
    )(tokens, norm_gain[None, :], ids, gates, w_gate, w_up, w_down)


def step(mesh, *arrays):
    tokens, norm_gain, w_gate, w_up, w_down, expert_ids, gate_weights = arrays
    ep_count, tp_count = mesh.shape["ep"], mesh.shape["tp"]
    rows, top_count = expert_ids.shape
    experts_all = ep_count * w_gate.shape[0]
    capacity = min(rows, rows * top_count * 4 // (3 * experts_all))
    dense = (
        w_gate.shape[0] == 1
        and tp_count == 2
        and ep_count % CORES == 0
        and ep_count > CORES
        and rows <= 2 * capacity
        and rows % (32 * PIECES) == 0
        and rows % (16 * SPLIT) == 0
    )
    return fused(*arrays) if dense else body(*arrays)


def solution(mesh):
    placed = (
        P(("grp", "ep"), None),
        P(),
        P("ep", None, "tp"),
        P("ep", None, "tp"),
        P("ep", "tp", None),
        P(("grp", "ep"), None),
        P(("grp", "ep"), None),
    )
    return jax.shard_map(
        functools.partial(step, mesh), mesh=mesh, in_specs=placed, out_specs=P(("grp", "ep"), "tp"), check_vma=False
    )
```

time: 88.4 us -> 73.3 us (0.83)
  Pallas kernels: 86.2 us -> 68.8 us
  local copies, waits for them, and re-layouts: 1.77 us -> 4.32 us
    pallas_call x1, Pallas kernels: 86.2 us -> 68.8 us  [fused(): pl.pallas_call(functools.partial(fused_kernel, chips), out_shape=jax.Shap...]
    pad x0 -> x2, local copies, waits for them, and re-layouts: none -> 2.56 us  [the longest x1 1.28 us: fused(): ids = jnp.pad(expert_ids.T, ((0, 0), (0, lanes)), constant_values=-1)]
where the time goes in v1:
time: 73.3 us; the launch traced here: 73.1 us
  Pallas kernels  68.8 us (94%)
  local copies, waits for them, and re-layouts  4.32 us (6%)
    pallas_call x1, Pallas kernels, fused(): pl.pallas_call(functools.partial(fused_kernel, chips), out_shape=jax.Shap...  68.8 us
    unnamed x1, local copies, waits for them, and re-layouts  1.77 us

profile of v1, /device:TPU:0, one launch (start us, length us, event | category | flops | bytes accessed | tf_op | source)
XLA Modules:
  0.0 73.1 jit_solution(18091712988291268965)
XLA Ops:
  0.0 1.3 %pad.8.ids_ref = s32[4,256]{1,0:T(4,128)} pad(s32[4,192]{1,0:T(4,128)} %bitcast.4, s32[]{:T(128)} %constant.1.clone.1), padding=0_0x0_64 | pad | bytes 7172 | tf_op jit(solution)/shard_map/jit(_pad)/pad | solution.py:479
  1.3 1.3 %pad.9.gates_ref = f32[4,256]{1,0:T(4,128)} pad(f32[4,192]{1,0:T(4,128)} %bitcast.5, f32[]{:T(128)} %constant.4.clone.1), padding=0_0x0_64 | pad | bytes 7172 | tf_op jit(solution)/shard_map/jit(_pad)/pad | solution.py:480
  2.6 68.8 %shard_map.73 = bf16[192,1024]{1,0:T(8,128)(2,1)} custom-call(bf16[192,2048]{1,0:T(8,128)(2,1)} %tok_ref.1, f32[1,2048]{1,0:T(1,128)} %bitcast.3, s32[4,256]{1,0:T(4,128)} %pad.8.ids_ref, f32[4,256]{1,0:T(4,128)} %pad.9.gates_ref, bf16[1,2048,512]{2,1,0:T(8,128)(2,1)} %wg_hbm.1, bf16[1,2048,512]{2,1,0:T(8,128)(2,1)} %wu_hbm.1, bf16[1,512,2048]{2,1,0:T(8,128)(2,1)} %wd_hbm.1), custom_call_target="tpu_custom_call" | custom-call | tf_op jit(solution)/shard_map/pallas_call | solution.py:481
  71.3 1.8 %copy.9 = bf16[192,1024]{1,0:T(8,128)(2,1)} copy(bf16[192,1024]{1,0:T(8,128)(2,1)} %shard_map.73) | data formatting | bytes 786432

commit v2 on v1

--- a/solution.py
+++ b/solution.py
@@ -62,7 +62,7 @@
 
 MESH = pl.DeviceIdType.MESH
 CORES = 2
-PIECES = 3
+PIECES = 6
 SPLIT = 3
 HIDDEN_TILE = 256
 COLUMN_TILE = 512
@@ -70,14 +70,18 @@
 
 def fused_kernel(
     chips,
+    tok_hbm,
+    gain_hbm,
+    ids_hbm,
+    gates_hbm,
+    wg_hbm,
+    wu_hbm,
+    wd_hbm,
+    out_ref,
     tok_ref,
     gain_ref,
     ids_ref,
     gates_ref,
-    wg_hbm,
-    wu_hbm,
-    wd_hbm,
-    out_ref,
     rows_all,
     codes,
     wg,
@@ -93,6 +97,7 @@
     far_out,
     far_in,
     agg_in,
+    input_sem,
     weight_sem,
     pair_sem,
     code_send,
@@ -108,7 +113,7 @@
 ):
     ep, tp = lax.axis_index("ep"), lax.axis_index("tp")
     z, core = lax.div(ep, CORES), lax.rem(ep, CORES)
-    rows, width = tok_ref.shape
+    rows, width = tok_hbm.shape
     half = rows // 2
     piece = half // PIECES
     out_width = width // 2
@@ -119,6 +124,21 @@
     onward = ({"ep": (z + 1) * CORES + core}, {"ep": (z - 1) * CORES + core})
     has_next = (z < last, z > 0)
 
+    def half_of(which):
+        return pl.ds(pl.multiple_of(which * half, 16), half)
+
+    small = [
+        pltpu.make_async_copy(source, target, input_sem.at[i])
+        for i, (source, target) in enumerate(
+            (
+                (gain_hbm, gain_ref),
+                (ids_hbm, ids_ref),
+                (gates_hbm, gates_ref),
+                (tok_hbm.at[half_of(tp)], tok_ref.at[half_of(tp)]),
+                (tok_hbm.at[half_of(1 - tp)], tok_ref.at[half_of(1 - tp)]),
+            )
+        )
+    ]
     sources = (wg_hbm.at[0], wu_hbm.at[0], wd_hbm.at[0])
     loads = [
         pltpu.make_async_copy(source, target, weight_sem.at[i])
@@ -126,8 +146,6 @@
             zip(sources, (wg.at[0], wu.at[0], wd.at[pl.ds(0, hidden)]))
         )
     ]
-    for load in loads:
-        load.start()
 
     barrier = pltpu.get_barrier_semaphore()
     for target in (partner, peer):
@@ -137,6 +155,9 @@
         @pl.when(has_next[side])
         def _(side=side):
             pl.semaphore_signal(barrier, inc=1, device_id=onward[side], device_id_type=MESH)
+
+    for load in small + loads:
+        load.start()
 
     def block_at(side, distance):
         return z - distance if side == 0 else z + distance
@@ -164,18 +185,21 @@
         )
     ]
 
-    def normed(start):
-        span = pl.ds(pl.multiple_of(start, 16), half)
+    def normed(which):
+        span = half_of(which)
         widened = tok_ref[span].astype(jnp.float32)
         scaled = widened * lax.rsqrt(jnp.mean(widened * widened, axis=-1, keepdims=True) + epsilon)
         rows_all[z, span] = (scaled * gain_ref[...]).astype(jnp.bfloat16)
 
-    normed(tp * half)
-    line = lax.broadcasted_iota(jnp.int32, codes.shape[1:], 0)
-    gate = jnp.zeros(codes.shape[1:], jnp.float32)
+    for load in small[:4]:
+        load.wait()
+    normed(tp)
+    line = lax.broadcasted_iota(jnp.int32, (codes.shape[1], rows), 0)
+    gate = jnp.zeros(line.shape, jnp.float32)
     for k in range(ids_ref.shape[0]):
         gate = gate + jnp.where(line == ids_ref[k : k + 1, :], gates_ref[k : k + 1, :], 0.0)
-    codes[z] = gate
+    codes[z] = jnp.zeros(codes.shape[1:], jnp.float32)
+    codes[z, :, :rows] = gate
 
     neighbours = 2 + jnp.where(z > 0, 1, 0) + jnp.where(z < last, 1, 0)
     pl.semaphore_wait(barrier, neighbours)
@@ -221,9 +245,15 @@
 
     for give in gives:
         give.start()
-    normed((1 - tp) * half)
+    small[4].wait()
+    normed(1 - tp)
+
+    centre = jnp.where(2 * z < last, 1, 0)
+    is_centre = (centre == 0, centre == 1)
 
     def gather_z(distance, pieces):
+        if distance > last:
+            return
         for q in pieces:
             for side in range(2):
 
@@ -240,15 +270,41 @@
                             if q == 0:
                                 code_copy(side, distance, distance).start()
 
-                    x_copy(side, distance, q, tp).start()
-
-    def gather_x(distance):
-        for q in range(PIECES):
-            for side in range(2):
-
-                @pl.when(valid(side, distance))
-                def _(side=side, q=q):
-                    x_copy(side, distance, q, 1 - tp).wait_recv()
+                    if distance > 1:
+                        x_copy(side, distance, q, tp).start()
+                    else:
+
+                        @pl.when(is_centre[side])
+                        def _():
+                            x_copy(side, distance, q, tp).start()
+
+    def outer_x():
+        for side in range(2):
+
+            @pl.when(valid(side, 1) & jnp.logical_not(is_centre[side]))
+            def _(side=side):
+                for q in range(PIECES):
+                    x_copy(side, 1, q, tp).start()
+
+    def in_turn(distance, turn):
+        side = centre if turn == 0 else 1 - centre
+        block = z + distance * (2 * side - 1)
+        return side, block, (block >= 0) & (block < chips)
+
+    def wait_x(distance, turn):
+        side, block, there = in_turn(distance, turn)
+
+        @pl.when(there)
+        def _():
+            for q in range(PIECES):
+                ref = rows_of(block, 1 - tp, q)
+                remote(
+                    ref,
+                    ref,
+                    x_send.at[side, distance - 1, q],
+                    x_recv.at[side, distance - 1, q],
+                    peer,
+                ).wait_recv()
 
     theirs = pl.multiple_of((1 - tp) * out_width, 128)
     mine = pl.multiple_of(tp * out_width, 128)
@@ -323,36 +379,42 @@
             ref, ref, far_send.at[side, 0, q], far_recv.at[side, distance - 1, q], peer
         )
 
-    def experts_at(distance):
-        def one(side, carry):
-            block = z + distance * (2 * side - 1)
-
-            @pl.when((block >= 0) & (block < chips))
-            def _():
-                activate(block, 0)
-                activate(block, 1)
-                if distance == 1:
-                    for start in range(0, width, COLUMN_TILE):
-                        merge_out[side, :, start : start + COLUMN_TILE] = project(start).astype(
-                            jnp.bfloat16
-                        )
-                    for q in range(SPLIT):
-                        merge_copy(side, 1 - side, q, block).start()
-                else:
-                    for start in range(0, out_width, COLUMN_TILE):
-                        side_out[block, :, start : start + COLUMN_TILE] = project(
-                            pl.multiple_of(theirs + start, 128)
-                        ).astype(jnp.bfloat16)
-                    for q in range(SPLIT):
-                        side_copy(block, q).start()
-                    for start in range(0, out_width, COLUMN_TILE):
-                        part[block, :, start : start + COLUMN_TILE] = project(
-                            pl.multiple_of(mine + start, 128)
-                        )
-
-            return carry
-
-        lax.fori_loop(0, 2, one, 0)
+    def hidden_at(distance, turn, slot):
+        side, block, there = in_turn(distance, turn)
+
+        @pl.when(there)
+        def _():
+            activate(block, slot)
+
+    def project_at(distance, turn):
+        side, block, there = in_turn(distance, turn)
+
+        @pl.when(there)
+        def _():
+            if distance == 1:
+                for start in range(0, width, COLUMN_TILE):
+                    merge_out[side, :, start : start + COLUMN_TILE] = project(start).astype(
+                        jnp.bfloat16
+                    )
+                for q in range(SPLIT):
+                    merge_copy(side, 1 - side, q, block).start()
+            else:
+                for start in range(0, out_width, COLUMN_TILE):
+                    side_out[block, :, start : start + COLUMN_TILE] = project(
+                        pl.multiple_of(theirs + start, 128)
+                    ).astype(jnp.bfloat16)
+                for start in range(0, out_width, COLUMN_TILE):
+                    part[block, :, start : start + COLUMN_TILE] = project(
+                        pl.multiple_of(mine + start, 128)
+                    )
+
+    def sides_at(distance, turn):
+        side, block, there = in_turn(distance, turn)
+
+        @pl.when(there)
+        def _():
+            for q in range(SPLIT):
+                side_copy(block, q).start()
 
     def far_sum(side, distance, more):
         block = block_at(side, distance)
@@ -404,24 +466,44 @@
 
             out_ref[span] = part[z, span].astype(jnp.bfloat16)
 
-    for load in loads:
+    third = PIECES // 3
+
+    def pieces_of(distance, first, count):
+        gather_z(distance, range(first * third, (first + count) * third))
+
+    for load in loads[:2]:
         load.wait()
+    gather_z(1, range(0, 1))
     activate(z, 0)
-    gather_z(1, range(PIECES - 1))
+    gather_z(1, range(1, 2 * third))
     for give in gives[:2]:
         give.wait_recv()
     activate(z, 1)
-    gather_z(1, range(PIECES - 1, PIECES))
+    pieces_of(1, 2, 1)
+    outer_x()
+    loads[2].wait()
     gives[2].wait_recv()
     for start in range(0, width, COLUMN_TILE):
         kept[:, start : start + COLUMN_TILE] = project(start)
-    if last >= 2:
-        gather_z(2, range(PIECES))
-    for turn in range(1, last + 1):
-        gather_x(turn)
-        experts_at(turn)
-        if turn + 2 <= last:
-            gather_z(turn + 2, range(PIECES))
+    for distance in range(1, chips):
+        for turn in range(2):
+            if 2 * distance + turn > chips and turn == 1:
+                continue
+            first = turn == 0
+            if first:
+                gather_z(distance + 1, range(0, 1))
+            wait_x(distance, turn)
+            hidden_at(distance, turn, 0)
+            if first:
+                gather_z(distance + 1, range(1, third))
+            hidden_at(distance, turn, 1)
+            if first:
+                pieces_of(distance + 1, 1, 1)
+            project_at(distance, turn)
+            if first:
+                pieces_of(distance + 1, 2, 1)
+            if distance > 1:
+                sides_at(distance, turn)
     for distance in range(2, last):
         far_sums(distance, False)
     own_exchange()
@@ -466,6 +548,7 @@
 
 def fused(tokens, norm_gain, w_gate, w_up, w_down, expert_ids, gate_weights):
     rows, width = tokens.shape
+    top_count = expert_ids.shape[1]
     chips = lax.axis_size("ep") // CORES
     experts_all = chips * CORES
     hidden = w_gate.shape[2]
@@ -476,14 +559,16 @@
     vmem = pl.BlockSpec(memory_space=pltpu.VMEM)
     anywhere = pl.BlockSpec(memory_space=pl.ANY)
     dma = pltpu.SemaphoreType.DMA
-    ids = jnp.pad(expert_ids.T, ((0, 0), (0, lanes)), constant_values=-1)
-    gates = jnp.pad(gate_weights.T, ((0, 0), (0, lanes)))
     return pl.pallas_call(
         functools.partial(fused_kernel, chips),
         out_shape=jax.ShapeDtypeStruct((rows, out_width), jnp.bfloat16),
-        in_specs=[vmem] * 4 + [anywhere] * 3,
+        in_specs=[anywhere] * 7,
         out_specs=vmem,
         scratch_shapes=[
+            pltpu.VMEM((rows, width), jnp.bfloat16),
+            pltpu.VMEM((1, width), jnp.float32),
+            pltpu.VMEM((top_count, rows), jnp.int32),
+            pltpu.VMEM((top_count, rows), jnp.float32),
             pltpu.VMEM((chips, rows, width), jnp.bfloat16),
             pltpu.VMEM((chips, experts_all + -experts_all % 8, rows + lanes), jnp.float32),
             pltpu.VMEM((CORES, width, hidden), jnp.bfloat16),
@@ -499,6 +584,7 @@
             pltpu.VMEM((chips, rows, out_width), jnp.bfloat16),
             pltpu.VMEM((2, rows, out_width), jnp.bfloat16),
             pltpu.VMEM((2, hops, rows, out_width), jnp.bfloat16),
+            dma((5,)),
             dma((3,)),
             dma((2, 3)),
             dma((2, last)),
@@ -513,7 +599,7 @@
             dma((2, hops + 1, SPLIT)),
         ],
         compiler_params=pltpu.CompilerParams(collective_id=0, has_side_effects=True),
-    )(tokens, norm_gain[None, :], ids, gates, w_gate, w_up, w_down)
+    )(tokens, norm_gain[None, :], expert_ids.T, gate_weights.T, w_gate, w_up, w_down)
 
 
 def step(mesh, *arrays):

time: 73.3 us -> 70.5 us (0.962)
  local copies, waits for them, and re-layouts: 4.32 us -> 1.77 us
    pad x2 -> x0, local copies, waits for them, and re-layouts: 2.56 us -> none  [the longest x1 1.28 us: fused(): ids = jnp.pad(expert_ids.T, ((0, 0), (0, lanes)), constant_values=-1)]
where the time goes in v2:
time: 70.5 us; the launch traced here: 70.3 us
  Pallas kernels  68.6 us (97%)
  local copies, waits for them, and re-layouts  1.77 us (3%)
    pallas_call x1, Pallas kernels, fused(): pl.pallas_call(functools.partial(fused_kernel, chips), out_shape=jax.Shap...  68.6 us
    unnamed x1, local copies, waits for them, and re-layouts  1.77 us

profile of v2, /device:TPU:0, one launch (start us, length us, event | category | flops | bytes accessed | tf_op | source)
XLA Modules:
  0.0 70.3 jit_solution(13813485950492186515)
XLA Ops:
  0.0 68.6 %shard_map.73 = bf16[192,1024]{1,0:T(8,128)(2,1)} custom-call(bf16[192,2048]{1,0:T(8,128)(2,1)} %tok_hbm.1, f32[1,2048]{1,0:T(1,128)} %bitcast.3, s32[4,192]{1,0:T(4,128)} %bitcast.4, f32[4,192]{1,0:T(4,128)} %bitcast.5, bf16[1,2048,512]{2,1,0:T(8,128)(2,1)} %wg_hbm.1, bf16[1,2048,512]{2,1,0:T(8,128)(2,1)} %wu_hbm.1, bf16[1,512,2048]{2,1,0:T(8,128)(2,1)} %wd_hbm.1), custom_call_target="tpu_custom_call" | custom-call | tf_op jit(solution)/shard_map/pallas_call | solution.py:562
  68.6 1.8 %copy.9 = bf16[192,1024]{1,0:T(8,128)(2,1)} copy(bf16[192,1024]{1,0:T(8,128)(2,1)} %shard_map.73) | data formatting | bytes 786432

commit v3 on v2

--- a/solution.py
+++ b/solution.py
@@ -64,6 +64,7 @@
 CORES = 2
 PIECES = 6
 SPLIT = 3
+OVER = 1
 HIDDEN_TILE = 256
 COLUMN_TILE = 512
 
@@ -97,6 +98,7 @@
     far_out,
     far_in,
     agg_in,
+    over_in,
     input_sem,
     weight_sem,
     pair_sem,
@@ -110,6 +112,7 @@
     side_sem,
     far_send,
     far_recv,
+    over_sem,
 ):
     ep, tp = lax.axis_index("ep"), lax.axis_index("tp")
     z, core = lax.div(ep, CORES), lax.rem(ep, CORES)
@@ -123,6 +126,7 @@
     peer = {"tp": 1 - tp}
     onward = ({"ep": (z + 1) * CORES + core}, {"ep": (z - 1) * CORES + core})
     has_next = (z < last, z > 0)
+    centre = jnp.where(2 * z < last, 1, 0)
 
     def half_of(which):
         return pl.ds(pl.multiple_of(which * half, 16), half)
@@ -208,83 +212,80 @@
         start = pl.multiple_of(which * half + q * piece, 16)
         return rows_all.at[block, pl.ds(start, piece), :]
 
-    def z_copy(side, distance, q):
-        ref = rows_of(block_at(side, distance), tp, q)
-        return remote(
-            ref, ref, z_send.at[side, distance, q], z_recv.at[side, distance, q], onward[side]
-        )
-
-    def z_arrival(side, distance, q):
-        ref = rows_of(block_at(side, distance), tp, q)
-        return remote(
-            ref,
-            ref,
-            z_send.at[side, distance - 1, q],
-            z_recv.at[side, distance - 1, q],
-            onward[side],
-        )
-
-    def code_copy(side, distance, hop):
-        ref = codes.at[block_at(side, distance)]
-        return remote(ref, ref, code_send.at[side, hop], code_recv.at[side, hop], onward[side])
-
-    def x_copy(side, distance, q, which):
-        ref = rows_of(block_at(side, distance), which, q)
+    def flow(turn):
+        side = centre if turn == 0 else 1 - centre
+        ahead = z + 1 - 2 * side
+        return side, {"ep": ahead * CORES + core}, (ahead >= 0) & (ahead < chips)
+
+    def at(turn, distance):
+        block = z + distance * (2 * flow(turn)[0] - 1)
+        return block, (block >= 0) & (block < chips)
+
+    def z_copy(turn, distance, q):
+        side, device, _ = flow(turn)
+        ref = rows_of(at(turn, distance)[0], tp, q)
+        return remote(ref, ref, z_send.at[side, distance, q], z_recv.at[side, distance, q], device)
+
+    def z_arrival(turn, distance, q):
+        side, device, _ = flow(turn)
+        ref = rows_of(at(turn, distance)[0], tp, q)
+        return remote(
+            ref, ref, z_send.at[side, distance - 1, q], z_recv.at[side, distance - 1, q], device
+        )
+
+    def code_copy(turn, distance, hop):
+        side, device, _ = flow(turn)
+        ref = codes.at[at(turn, distance)[0]]
+        return remote(ref, ref, code_send.at[side, hop], code_recv.at[side, hop], device)
+
+    def x_copy(turn, distance, q, which):
+        side = flow(turn)[0]
+        ref = rows_of(at(turn, distance)[0], which, q)
         return remote(
             ref, ref, x_send.at[side, distance - 1, q], x_recv.at[side, distance - 1, q], peer
         )
 
     for q in range(PIECES):
-        for side in range(2):
-
-            @pl.when(has_next[side])
-            def _(side=side, q=q):
-                z_copy(side, 0, q).start()
+        for turn in range(2):
+
+            @pl.when(flow(turn)[2])
+            def _(turn=turn, q=q):
+                z_copy(turn, 0, q).start()
                 if q == 0:
-                    code_copy(side, 0, 0).start()
+                    code_copy(turn, 0, 0).start()
 
     for give in gives:
         give.start()
     small[4].wait()
     normed(1 - tp)
 
-    centre = jnp.where(2 * z < last, 1, 0)
-    is_centre = (centre == 0, centre == 1)
-
     def gather_z(distance, pieces):
         if distance > last:
             return
         for q in pieces:
-            for side in range(2):
-
-                @pl.when(valid(side, distance))
-                def _(side=side, q=q):
-                    z_arrival(side, distance, q).wait_recv()
+            for turn in range(2):
+
+                @pl.when(at(turn, distance)[1])
+                def _(turn=turn, q=q):
+                    z_arrival(turn, distance, q).wait_recv()
                     if q == 0:
-                        code_copy(side, distance, distance - 1).wait_recv()
+                        code_copy(turn, distance, distance - 1).wait_recv()
                     if distance < last:
 
-                        @pl.when(has_next[side])
+                        @pl.when(flow(turn)[2])
                         def _():
-                            z_copy(side, distance, q).start()
+                            z_copy(turn, distance, q).start()
                             if q == 0:
-                                code_copy(side, distance, distance).start()
-
-                    if distance > 1:
-                        x_copy(side, distance, q, tp).start()
-                    else:
-
-                        @pl.when(is_centre[side])
-                        def _():
-                            x_copy(side, distance, q, tp).start()
+                                code_copy(turn, distance, distance).start()
+
+                    if distance > 1 or turn == 0:
+                        x_copy(turn, distance, q, tp).start()
 
     def outer_x():
-        for side in range(2):
-
-            @pl.when(valid(side, 1) & jnp.logical_not(is_centre[side]))
-            def _(side=side):
-                for q in range(PIECES):
-                    x_copy(side, 1, q, tp).start()
+        @pl.when(at(1, 1)[1])
+        def _():
+            for q in range(PIECES):
+                x_copy(1, 1, q, tp).start()
 
     def in_turn(distance, turn):
         side = centre if turn == 0 else 1 - centre
@@ -292,19 +293,10 @@
         return side, block, (block >= 0) & (block < chips)
 
     def wait_x(distance, turn):
-        side, block, there = in_turn(distance, turn)
-
-        @pl.when(there)
+        @pl.when(at(turn, distance)[1])
         def _():
             for q in range(PIECES):
-                ref = rows_of(block, 1 - tp, q)
-                remote(
-                    ref,
-                    ref,
-                    x_send.at[side, distance - 1, q],
-                    x_recv.at[side, distance - 1, q],
-                    peer,
-                ).wait_recv()
+                x_copy(turn, distance, q, 1 - tp).wait_recv()
 
     theirs = pl.multiple_of((1 - tp) * out_width, 128)
     mine = pl.multiple_of(tp * out_width, 128)
@@ -363,6 +355,24 @@
             receiver = far_recv.at[side, distance - 2, q]
             device = onward[1 - side]
         return remote(far_out.at[dest, span_of(q)], target, sender, receiver, device)
+
+    def over_copy(side, block, q):
+        return remote(
+            side_out.at[block, span_of(q)],
+            over_in.at[1 - side, span_of(q)],
+            over_sem.at[0, side, q],
+            over_sem.at[1, 1 - side, q],
+            chip_of(block),
+        )
+
+    def last_copy(side, block, q):
+        return remote(
+            far_out.at[block, span_of(q)],
+            far_in.at[1 - side, span_of(q)],
+            far_send.at[side, 0, q],
+            far_recv.at[1 - side, 0, q],
+            chip_of(block),
+        )
 
     def far_arrival(side, q):
         return remote(
@@ -410,15 +420,29 @@
 
     def sides_at(distance, turn):
         side, block, there = in_turn(distance, turn)
+        over = OVER if distance == 2 else 0
+        through = flow(turn)[2]
+
+        @pl.when(there & jnp.logical_not(through))
+        def _():
+            for q in range(over):
+                over_copy(side, block, q).start()
+                far_out[block, span_of(q)] = part[block, span_of(q)].astype(jnp.bfloat16)
+                last_copy(side, block, q).start()
+
+        @pl.when(there & through)
+        def _():
+            for q in range(over):
+                side_copy(block, q).start()
 
         @pl.when(there)
         def _():
-            for q in range(SPLIT):
+            for q in range(over, SPLIT):
                 side_copy(block, q).start()
 
     def far_sum(side, distance, more):
         block = block_at(side, distance)
-        for q in range(SPLIT):
+        for q in range(OVER if distance == 2 and not more else 0, SPLIT):
             span = span_of(q)
             side_copy(block, q).wait_recv()
             total = part[block, span] + side_in[block, span].astype(jnp.float32)
@@ -445,6 +469,15 @@
                 def _(side=side, q=q):
                     merge_copy(1 - side, side, q, block_at(side, 1)).wait_recv()
                     kept[span] = kept[span] + merge_in[side, span].astype(jnp.float32)
+
+            if q < OVER and chips > 2:
+                for side in range(2):
+
+                    @pl.when((z == 2) if side == 0 else (z + 2 == last))
+                    def _(side=side, q=q):
+                        over_copy(1 - side, block_at(side, 2), q).wait_recv()
+                        here = (span, pl.ds(theirs, out_width))
+                        kept[here] = kept[here] + over_in[side, span].astype(jnp.float32)
 
             side_out[z, span] = kept[span, pl.ds(theirs, out_width)].astype(jnp.bfloat16)
             side_copy(z, q).start()
@@ -511,39 +544,55 @@
         far_sums(last, False)
     for distance in range(last - 1, 1, -1):
         far_sums(distance, True)
-    finish()
-
     for give in gives:
         give.wait_send()
     for q in range(PIECES):
-        for side in range(2):
+        for turn in range(2):
             for distance in range(chips):
                 if distance < last:
 
-                    @pl.when(valid(side, distance) & has_next[side])
+                    @pl.when(at(turn, distance)[1] & flow(turn)[2])
+                    def _(turn=turn, distance=distance, q=q):
+                        z_copy(turn, distance, q).wait_send()
+                        if q == 0:
+                            code_copy(turn, distance, distance).wait_send()
+
+                if distance > 0:
+
+                    @pl.when(at(turn, distance)[1])
+                    def _(turn=turn, distance=distance, q=q):
+                        x_copy(turn, distance, q, tp).wait_send()
+
+    for q in range(SPLIT):
+        for side in range(2):
+
+            @pl.when(valid(side, 1))
+            def _(side=side, q=q):
+                merge_copy(side, 1 - side, q, block_at(side, 1)).wait_send()
+
+            for distance in range(2, chips):
+                over = distance == 2 and q < OVER
+                through = has_next[side] if over else True
+
+                @pl.when(valid(side, distance) & through)
+                def _(side=side, distance=distance, q=q):
+                    side_copy(block_at(side, distance), q).wait_send()
+
+                if over:
+
+                    @pl.when(valid(side, distance) & jnp.logical_not(has_next[side]))
                     def _(side=side, distance=distance, q=q):
-                        z_copy(side, distance, q).wait_send()
-                        if q == 0:
-                            code_copy(side, distance, distance).wait_send()
-
-                if distance > 0:
-
-                    @pl.when(valid(side, distance))
-                    def _(side=side, distance=distance, q=q):
-                        x_copy(side, distance, q, tp).wait_send()
-
+                        over_copy(side, block_at(side, distance), q).wait_send()
+
+    finish()
     for q in range(SPLIT):
         side_copy(z, q).wait_send()
         for side in range(2):
-            for distance in range(1, chips):
+            for distance in range(2, chips):
 
                 @pl.when(valid(side, distance))
                 def _(side=side, distance=distance, q=q):
-                    if distance == 1:
-                        merge_copy(side, 1 - side, q, block_at(side, 1)).wait_send()
-                    else:
-                        side_copy(block_at(side, distance), q).wait_send()
-                        far_copy(side, distance, q).wait_send()
+                    far_copy(side, distance, q).wait_send()
 
 
 def fused(tokens, norm_gain, w_gate, w_up, w_down, expert_ids, gate_weights):
@@ -561,7 +610,7 @@
     dma = pltpu.SemaphoreType.DMA
     return pl.pallas_call(
         functools.partial(fused_kernel, chips),
-        out_shape=jax.ShapeDtypeStruct((rows, out_width), jnp.bfloat16),
+        out_shape=pltpu.VMEM((rows, out_width), jnp.bfloat16),
         in_specs=[anywhere] * 7,
         out_specs=vmem,
         scratch_shapes=[
@@ -584,6 +633,7 @@
             pltpu.VMEM((chips, rows, out_width), jnp.bfloat16),
             pltpu.VMEM((2, rows, out_width), jnp.bfloat16),
             pltpu.VMEM((2, hops, rows, out_width), jnp.bfloat16),
+            pltpu.VMEM((2, rows, out_width), jnp.bfloat16),
             dma((5,)),
             dma((3,)),
             dma((2, 3)),
@@ -597,6 +647,7 @@
             dma((2, chips, SPLIT)),
             dma((2, hops, SPLIT)),
             dma((2, hops + 1, SPLIT)),
+            dma((2, 2, SPLIT)),
         ],
         compiler_params=pltpu.CompilerParams(collective_id=0, has_side_effects=True),
     )(tokens, norm_gain[None, :], expert_ids.T, gate_weights.T, w_gate, w_up, w_down)

time: 70.5 us -> 68.4 us (0.970)
  Pallas kernels: 68.6 us -> 67.4 us
  local copies, waits for them, and re-layouts: 1.77 us -> 0.75 us
    pallas_call x1, Pallas kernels: 68.6 us -> 67.4 us  [fused(): pl.pallas_call(functools.partial(fused_kernel, chips), out_shape=pltpu.VM...]
    unnamed x1, local copies, waits for them, and re-layouts: 1.77 us -> 0.75 us
where the time goes in v3:
time: 68.4 us; the launch traced here: 68.2 us
  Pallas kernels  67.4 us (99%)
  local copies, waits for them, and re-layouts  0.75 us (1%)
    pallas_call x1, Pallas kernels, fused(): pl.pallas_call(functools.partial(fused_kernel, chips), out_shape=pltpu.VM...  67.4 us

profile of v3, /device:TPU:0, one launch (start us, length us, event | category | flops | bytes accessed | tf_op | source)
XLA Modules:
  0.0 68.2 jit_solution(1315352274405336752)
XLA Ops:
  0.0 67.4 %shard_map.73 = bf16[192,1024]{1,0:T(8,128)(2,1)S(1)} custom-call(bf16[192,2048]{1,0:T(8,128)(2,1)} %tok_hbm.1, f32[1,2048]{1,0:T(1,128)} %bitcast.3, s32[4,192]{1,0:T(4,128)} %bitcast.4, f32[4,192]{1,0:T(4,128)} %bitcast.5, bf16[1,2048,512]{2,1,0:T(8,128)(2,1)} %wg_hbm.1, bf16[1,2048,512]{2,1,0:T(8,128)(2,1)} %wu_hbm.1, bf16[1,512,2048]{2,1,0:T(8,128)(2,1)} %wd_hbm.1), custom_call_target="tpu_custom_call" | custom-call | tf_op jit(solution)/shard_map/pallas_call | solution.py:611
  67.4 0.7 %copy.9 = bf16[192,1024]{1,0:T(8,128)(2,1)} copy(bf16[192,1024]{1,0:T(8,128)(2,1)S(1)} %shard_map.73) | data formatting | bytes 786432

commit v4 on v2

v4 whole, which is shorter than its diff:
```python
import functools

import jax
import jax.numpy as jnp
from jax import lax
from jax.experimental import pallas as pl
from jax.experimental.pallas import tpu as pltpu
from jax.sharding import PartitionSpec as P

epsilon = 1e-06
clamp_limit = 7.0
swish_alpha = 1.702


def rms_norm(tokens, norm_gain):
    widened = tokens.astype(jnp.float32)
    scaled = widened * lax.rsqrt(jnp.mean(widened * widened, axis=-1, keepdims=True) + epsilon)
    return (scaled * norm_gain).astype(jnp.bfloat16)


def body(tokens, norm_gain, w_gate, w_up, w_down, expert_ids, gate_weights):
    tok_rows, model_width = tokens.shape
    top_count = expert_ids.shape[1]
    ep_count = lax.axis_size("ep")
    local_experts = w_gate.shape[0]
    experts_all = local_experts * ep_count
    capacity = min(tok_rows, tok_rows * top_count * 4 // (3 * experts_all))
    normed = rms_norm(tokens, norm_gain)
    flat_ids = expert_ids.reshape(-1)
    onehot = (flat_ids[:, None] == jnp.arange(experts_all, dtype=jnp.int32)[None, :]).astype(
        jnp.int32
    )
    before = jnp.cumsum(onehot, axis=0) - onehot
    slot_index = jnp.sum(before * onehot, axis=1)
    dest_row = flat_ids * capacity + slot_index
    owner_tok = jnp.arange(tok_rows * top_count, dtype=jnp.int32) // top_count
    slot_table = (
        jnp.full((experts_all * capacity,), tok_rows, jnp.int32).at[dest_row].set(owner_tok)
    )
    padded = jnp.concatenate([normed, jnp.zeros((1, model_width), jnp.bfloat16)], axis=0)
    send_buffer = padded[slot_table].reshape(experts_all, capacity, model_width)
    received = lax.all_to_all(send_buffer, "ep", split_axis=0, concat_axis=0, tiled=True)
    expert_rows = received.reshape(ep_count, local_experts, capacity, model_width)
    gate_pre = jnp.einsum("sjcd,jdf->sjcf", expert_rows, w_gate, preferred_element_type=jnp.float32)
    up_pre = jnp.einsum("sjcd,jdf->sjcf", expert_rows, w_up, preferred_element_type=jnp.float32)
    gated = jnp.minimum(gate_pre, clamp_limit)
    linear = jnp.clip(up_pre, -clamp_limit, clamp_limit)
    activated = (gated * jax.nn.sigmoid(swish_alpha * gated) * (linear + 1.0)).astype(jnp.bfloat16)
    partial_value = jnp.einsum(
        "sjcf,jfd->sjcd", activated, w_down, preferred_element_type=jnp.float32
    ).astype(jnp.bfloat16)
    summed = (
        lax.psum_scatter(partial_value, "tp", scatter_dimension=3, tiled=True)
        .astype(jnp.float32)
        .astype(jnp.bfloat16)
    )
    returned = lax.all_to_all(summed, "ep", split_axis=0, concat_axis=0, tiled=True)
    returned = returned.reshape(experts_all * capacity, returned.shape[3])
    picked = returned[dest_row].reshape(tok_rows, top_count, returned.shape[1]).astype(jnp.float32)
    return jnp.sum(picked * gate_weights[:, :, None], axis=1).astype(jnp.bfloat16)


MESH = pl.DeviceIdType.MESH
CORES = 2
PIECES = (0, 1, 3, 5, 6)
SPANS = (0, 1, 3)
OVER = 1
HIDDEN_TILE = 256
COLUMN_TILE = 512


def fused_kernel(
    chips,
    tok_hbm,
    gain_hbm,
    ids_hbm,
    gates_hbm,
    wg_hbm,
    wu_hbm,
    wd_hbm,
    out_ref,
    tok_ref,
    gain_ref,
    ids_ref,
    gates_ref,
    rows_all,
    codes,
    gate_cols,
    wg,
    wu,
    wd,
    act,
    kept,
    part,
    merge_out,
    merge_in,
    side_out,
    side_in,
    far_out,
    far_in,
    agg_in,
    over_in,
    input_sem,
    weight_sem,
    pair_sem,
    code_send,
    code_recv,
    z_send,
    z_recv,
    x_send,
    x_recv,
    merge_send,
    merge_recv,
    side_send,
    side_recv,
    far_send,
    far_recv,
    agg_recv,
    over_send,
    over_recv,
):
    ep, tp = lax.axis_index("ep"), lax.axis_index("tp")
    z, core = lax.div(ep, CORES), lax.rem(ep, CORES)
    rows, width = tok_hbm.shape
    half = rows // 2
    out_width = width // 2
    hidden = wg.shape[2]
    last = chips - 1
    partner = {"ep": z * CORES + 1 - core}
    peer = {"tp": 1 - tp}
    centre = jnp.where(2 * z < last, 1, 0)

    def chip_of(block):
        return {"ep": block * CORES + core}

    def within(block):
        return (block >= 0) & (block < chips)

    def flow(turn):
        side = centre if turn == 0 else 1 - centre
        ahead = z + 1 - 2 * side
        return side, ahead, within(ahead)

    def at(turn, distance):
        block = z + distance * (2 * flow(turn)[0] - 1)
        return block, within(block)

    def half_of(which):
        return pl.ds(pl.multiple_of(which * half, 16), half)

    small = [
        pltpu.make_async_copy(source, target, input_sem.at[i])
        for i, (source, target) in enumerate(
            (
                (gain_hbm, gain_ref),
                (ids_hbm, ids_ref),
                (gates_hbm, gates_ref),
                (tok_hbm.at[half_of(tp)], tok_ref.at[half_of(tp)]),
                (tok_hbm.at[half_of(1 - tp)], tok_ref.at[half_of(1 - tp)]),
            )
        )
    ]
    sources = (wg_hbm.at[0], wu_hbm.at[0], wd_hbm.at[0])
    loads = [
        pltpu.make_async_copy(source, target, weight_sem.at[i])
        for i, (source, target) in enumerate(
            zip(sources, (wg.at[0], wu.at[0], wd.at[pl.ds(0, hidden)]))
        )
    ]

    barrier = pltpu.get_barrier_semaphore()
    for target in (partner, peer):
        pl.semaphore_signal(barrier, inc=1, device_id=target, device_id_type=MESH)
    for turn in range(2):

        @pl.when(flow(turn)[2])
        def _(turn=turn):
            target = chip_of(flow(turn)[1])
            pl.semaphore_signal(barrier, inc=1, device_id=target, device_id_type=MESH)

    for load in small + loads:
        load.start()

    def remote(source, target, send, recv, device):
        return pltpu.make_async_remote_copy(
            src_ref=source,
            dst_ref=target,
            send_sem=send,
            recv_sem=recv,
            device_id=device,
            device_id_type=MESH,
        )

    gives = [
        remote(source, target, pair_sem.at[0, i], pair_sem.at[1, i], partner)
        for i, (source, target) in enumerate(
            zip(sources, (wg.at[1], wu.at[1], wd.at[pl.ds(hidden, hidden)]))
        )
    ]

    def normed(which):
        span = half_of(which)
        widened = tok_ref[span].astype(jnp.float32)
        scaled = widened * lax.rsqrt(jnp.mean(widened * widened, axis=-1, keepdims=True) + epsilon)
        rows_all[z, span] = (scaled * gain_ref[...]).astype(jnp.bfloat16)

    for load in small[:4]:
        load.wait()
    normed(tp)
    line = lax.broadcasted_iota(jnp.int32, (codes.shape[1], rows), 0)
    gate = jnp.zeros(line.shape, jnp.float32)
    for k in range(ids_ref.shape[0]):
        gate = gate + jnp.where(line == ids_ref[k : k + 1, :], gates_ref[k : k + 1, :], 0.0)
    codes[z] = jnp.zeros(codes.shape[1:], jnp.float32)
    codes[z, :, :rows] = gate

    neighbours = 2 + jnp.where(z > 0, 1, 0) + jnp.where(z < last, 1, 0)
    pl.semaphore_wait(barrier, neighbours)

    count = len(PIECES) - 1

    def rows_of(block, which, q):
        unit = half // PIECES[-1]
        start = pl.multiple_of(which * half + PIECES[q] * unit, 16)
        return rows_all.at[block, pl.ds(start, (PIECES[q + 1] - PIECES[q]) * unit)]

    def sender(turn, distance):
        side, _, _ = flow(turn)
        return jnp.where(side == 1, chips, z) if distance == 0 else at(turn, distance)[0]

    def z_copy(turn, distance, q):
        block = at(turn, distance)[0]
        ref = rows_of(block, tp, q)
        device = chip_of(flow(turn)[1])
        return remote(
            ref, ref, z_send.at[sender(turn, distance)], z_recv.at[block, q], device
        )

    def z_sent(turn, distance):
        ref = rows_all.at[z, half_of(tp)]
        return remote(ref, ref, z_send.at[sender(turn, distance)], z_recv.at[z, 0], peer)

    def code_copy(turn, distance):
        block = at(turn, distance)[0]
        device = chip_of(flow(turn)[1])
        return remote(
            codes.at[block],
            codes.at[block],
            code_send.at[sender(turn, distance)],
            code_recv.at[block],
            device,
        )

    def x_copy(block, which, q):
        ref = rows_of(block, which, q)
        return remote(ref, ref, x_send.at[block], x_recv.at[block], peer)

    def x_whole(block, which):
        ref = rows_all.at[block, half_of(which)]
        return remote(ref, ref, x_send.at[block], x_recv.at[block], peer)

    for q in range(count):
        for turn in range(2):

            @pl.when(flow(turn)[2])
            def _(turn=turn, q=q):
                z_copy(turn, 0, q).start()
                if q == 0:
                    code_copy(turn, 0).start()

    for give in gives:
        give.start()
    small[4].wait()
    normed(1 - tp)

    def gather_z(distance, q):
        for turn in range(2):

            @pl.when(at(turn, distance)[1])
            def _(turn=turn):
                z_copy(turn, distance, q).wait_recv()
                if q == 0:
                    code_copy(turn, distance).wait_recv()
                if distance < last:

                    @pl.when(flow(turn)[2])
                    def _():
                        z_copy(turn, distance, q).start()
                        if q == 0:
                            code_copy(turn, distance).start()

                if distance > 1 or turn == 0:
                    x_copy(at(turn, distance)[0], tp, q).start()

    waiting = [(distance, q) for distance in range(1, chips) for q in range(count)]

    def pump():
        if waiting:
            gather_z(*waiting.pop(0))

    def pump_all(distance):
        while waiting and waiting[0][0] <= distance:
            pump()

    def outer_x():
        @pl.when(at(1, 1)[1])
        def _():
            for q in range(count):
                x_copy(at(1, 1)[0], tp, q).start()

    def wait_x(distance, turn):
        @pl.when(at(turn, distance)[1])
        def _():
            x_whole(at(turn, distance)[0], 1 - tp).wait_recv()

    theirs = pl.multiple_of((1 - tp) * out_width, 128)
    mine = pl.multiple_of(tp * out_width, 128)
    parts = len(SPANS) - 1
    unit = half // SPANS[-1]
    first_half, second_half = tp, 1 - tp

    def span_of(which, s):
        start = pl.multiple_of(which * half + SPANS[s] * unit, 16)
        return pl.ds(start, (SPANS[s + 1] - SPANS[s]) * unit)

    def activate(block, start, size, slot):
        if slot == 0:
            gate_cols[...] = jnp.transpose(codes[block])
        span = pl.ds(start, size)
        turned = gate_cols[span]
        lane = lax.broadcasted_iota(jnp.int32, turned.shape, 1)
        owner = ep if slot == 0 else z * CORES + 1 - core
        weight = jnp.sum(jnp.where(lane == owner, turned, 0.0), axis=1, keepdims=True)
        held = rows_all[block, span]
        for begin in range(0, hidden, HIDDEN_TILE):
            columns = slice(begin, begin + HIDDEN_TILE)
            gate_pre = jnp.dot(held, wg[slot, :, columns], preferred_element_type=jnp.float32)
            up_pre = jnp.dot(held, wu[slot, :, columns], preferred_element_type=jnp.float32)
            gated = jnp.minimum(gate_pre, clamp_limit)
            linear = jnp.clip(up_pre, -clamp_limit, clamp_limit)
            value = gated * jax.nn.sigmoid(swish_alpha * gated) * (linear + 1.0) * weight
            act[:size, slot * hidden + begin : slot * hidden + begin + HIDDEN_TILE] = value.astype(
                jnp.bfloat16
            )

    def project(start, size):
        return jnp.dot(
            act[:size], wd[:, pl.ds(start, COLUMN_TILE)], preferred_element_type=jnp.float32
        )

    def merge_copy(side, other, which, s, block):
        span = span_of(which, s)
        return remote(
            merge_out.at[side, span],
            merge_in.at[other, span],
            merge_send.at[side],
            merge_recv.at[other, which * parts + s],
            chip_of(block),
        )

    def side_copy(block, which, s):
        span = span_of(which, s)
        return remote(
            side_out.at[block, span],
            side_in.at[block, span],
            side_send.at[block],
            side_recv.at[block, which * parts + s],
            peer,
        )

    def over_copy(side, block, which, s):
        span = span_of(which, s)
        return remote(
            side_out.at[block, span],
            over_in.at[1 - side, span],
            over_send.at[side],
            over_recv.at[1 - side, which * OVER + s],
            chip_of(block),
        )

    def far_copy(side, distance, block, which, s):
        span = span_of(which, s)
        if distance == 2:
            target = far_in.at[1 - side, span]
            receiver = far_recv.at[1 - side, which * parts + s]
            device = chip_of(block)
        else:
            target = agg_in.at[side, distance - 3, span]
            receiver = agg_recv.at[side, distance - 3, which * parts + s]
            device = chip_of(z + 2 * side - 1)
        return remote(far_out.at[block, span], target, far_send.at[block], receiver, device)

    def sent(ref, sem):
        return remote(ref, ref, sem, side_recv.at[0, 0], peer)

    def arrived(ref, sem):
        return remote(ref, ref, side_send.at[0], sem, peer)

    def job(distance, turn, which, pumped):
        block, there = at(turn, distance)
        side, _, through = flow(turn)
        start = pl.multiple_of(which * half, 16)

        @pl.when(there)
        def _():
            activate(block, start, half, 0)

        @pl.when(there)
        def _():
            activate(block, start, half, 1)

        if pumped:
            pump()

        @pl.when(there)
        def _():
            rows_here = half_of(which)
            if distance == 1:
                for begin in range(0, width, COLUMN_TILE):
                    merge_out[side, rows_here, begin : begin + COLUMN_TILE] = project(
                        begin, half
                    ).astype(jnp.bfloat16)
                if turn == 0 or which is second_half:
                    for s in range(parts):
                        merge_copy(side, 1 - side, which, s, block).start()
            else:
                for begin in range(0, out_width, COLUMN_TILE):
                    side_out[block, rows_here, begin : begin + COLUMN_TILE] = project(
                        pl.multiple_of(theirs + begin, 128), half
                    ).astype(jnp.bfloat16)
                if distance == last:
                    for s in range(OVER if distance == 2 else 0, parts):
                        side_copy(block, which, s).start()
                for begin in range(0, out_width, COLUMN_TILE):
                    part[block, rows_here, begin : begin + COLUMN_TILE] = project(
                        pl.multiple_of(mine + begin, 128), half
                    )
            if distance == 2:

                @pl.when(jnp.logical_not(through))
                def _():
                    for s in range(OVER):
                        span = span_of(which, s)
                        over_copy(side, block, which, s).start()
                        far_out[block, span] = part[block, span].astype(jnp.bfloat16)
                        far_copy(side, 2, block, which, s).start()

        if pumped:
            pump()

    def merges_at(turn, which):
        block, there = at(turn, 1)
        side = flow(turn)[0]

        @pl.when(there)
        def _():
            for s in range(parts):
                merge_copy(side, 1 - side, which, s, block).start()

    def sides_at(distance, turn, which, going):
        block, there = at(turn, distance)
        through = flow(turn)[2]

        @pl.when(there & (through if going else jnp.logical_not(through)))
        def _():
            for s in range(OVER if distance == 2 and not going else 0, parts):
                side_copy(block, which, s).start()

    def far_sums(distance, more):
        for turn in range(2):
            block, there = at(turn, distance)
            side, _, through = flow(turn)

            @pl.when(there & (through if more else jnp.logical_not(through)))
            def _(block=block, side=side):
                for which in (second_half, first_half):
                    for s in range(OVER if distance == 2 and not more else 0, parts):
                        span = span_of(which, s)
                        side_copy(block, which, s).wait_recv()
                        total = part[block, span] + side_in[block, span].astype(jnp.float32)
                        if more:
                            arrived(
                                agg_in.at[side, distance - 2, span],
                                agg_recv.at[side, distance - 2, which * parts + s],
                            ).wait_recv()
                            total = total + agg_in[side, distance - 2, span].astype(jnp.float32)
                        far_out[block, span] = total.astype(jnp.bfloat16)
                        far_copy(side, distance, block, which, s).start()

    def own_exchange():
        for which in (first_half, second_half):
            for s in range(parts):
                span = span_of(which, s)
                for turn in range(2):

                    @pl.when(at(turn, 1)[1])
                    def _(turn=turn):
                        side = flow(turn)[0]
                        arrived(
                            merge_in.at[side, span], merge_recv.at[side, which * parts + s]
                        ).wait_recv()
                        kept[span] = kept[span] + merge_in[side, span].astype(jnp.float32)

                    if s < OVER and chips > 2:
                        side = flow(turn)[0]
                        block = at(turn, 2)[0]

                        @pl.when(block == jnp.where(side == 1, last, 0))
                        def _(side=side):
                            arrived(
                                over_in.at[side, span], over_recv.at[side, which * OVER + s]
                            ).wait_recv()
                            here = (span, pl.ds(theirs, out_width))
                            kept[here] = kept[here] + over_in[side, span].astype(jnp.float32)

                side_out[z, span] = kept[span, pl.ds(theirs, out_width)].astype(jnp.bfloat16)
                side_copy(z, which, s).start()

    def finish():
        for which in (second_half, first_half):
            for s in range(parts):
                span = span_of(which, s)
                here = (span, pl.ds(mine, out_width))
                if chips > 2:
                    for turn in range(2):

                        @pl.when(at(turn, 2)[1])
                        def _(turn=turn):
                            side = flow(turn)[0]
                            arrived(
                                far_in.at[side, span], far_recv.at[side, which * parts + s]
                            ).wait_recv()
                            kept[here] = kept[here] + far_in[side, span].astype(jnp.float32)

                side_copy(z, which, s).wait_recv()
                out_ref[span] = (kept[here] + side_in[z, span].astype(jnp.float32)).astype(
                    jnp.bfloat16
                )

    for load in loads[:2]:
        load.wait()
    pump()
    activate(z, 0, rows, 0)
    for _ in range(count - 2):
        pump()
    for give in gives[:2]:
        give.wait_recv()
    activate(z, 0, rows, 1)
    pump_all(1)
    outer_x()
    loads[2].wait()
    gives[2].wait_recv()
    for begin in range(0, width, COLUMN_TILE):
        kept[:, begin : begin + COLUMN_TILE] = project(begin, rows)

    outer = range(1, last // 2 + 1)
    job(1, 0, first_half, True)
    for distance in range(1, chips):
        if distance in outer:
            job(distance, 1, first_half, False)
        wait_x(distance, 0)
        job(distance, 0, second_half, distance < last)
        if 1 < distance < last:
            sides_at(distance, 0, second_half, True)
        if distance < last:
            pump_all(distance + 1)
            if distance == 1:
                merges_at(1, first_half)
            job(distance + 1, 0, first_half, True)
            if distance + 1 < last:
                sides_at(distance + 1, 0, first_half, True)
            if 1 < distance:
                sides_at(distance, 0, first_half, False)
        if distance in outer:
            wait_x(distance, 1)
            job(distance, 1, second_half, False)
            if distance > 1:
                for which in (first_half, second_half):
                    for going in (True, False):
                        sides_at(distance, 1, which, going)
    for distance in range(last - 1, 1, -1):
        sides_at(distance, 0, second_half, False)
    if last > 1:
        far_sums(last, False)
    own_exchange()
    for distance in range(last - 1, 1, -1):
        far_sums(distance, False)
        far_sums(distance, True)

    for give in gives:
        give.wait_send()
    for turn in range(2):
        for distance in range(chips):
            if distance < last:

                @pl.when(at(turn, distance)[1] & flow(turn)[2])
                def _(turn=turn, distance=distance):
                    z_sent(turn, distance).wait_send()
                    code_copy(turn, distance).wait_send()

            if distance > 0:

                @pl.when(at(turn, distance)[1])
                def _(turn=turn, distance=distance):
                    x_whole(at(turn, distance)[0], tp).wait_send()

        @pl.when(at(turn, 1)[1])
        def _(turn=turn):
            side = flow(turn)[0]
            sent(merge_out.at[side], merge_send.at[side]).wait_send()

    finish()
    sent(side_out.at[z], side_send.at[z]).wait_send()
    short = 2 * SPANS[OVER] * unit
    for turn in range(2):
        side, _, through = flow(turn)
        for distance in range(2, chips):
            block, there = at(turn, distance)
            whole = there & through if distance == 2 else there

            @pl.when(whole)
            def _(block=block):
                sent(side_out.at[block], side_send.at[block]).wait_send()

            if distance == 2:

                @pl.when(there & jnp.logical_not(through))
                def _(block=block, side=side):
                    rest = side_out.at[block, pl.ds(0, rows - short)]
                    sent(rest, side_send.at[block]).wait_send()
                    sent(side_out.at[block, pl.ds(0, short)], over_send.at[side]).wait_send()

            @pl.when(there)
            def _(block=block):
                sent(far_out.at[block], far_send.at[block]).wait_send()


def fused(tokens, norm_gain, w_gate, w_up, w_down, expert_ids, gate_weights):
    rows, width = tokens.shape
    top_count = expert_ids.shape[1]
    chips = lax.axis_size("ep") // CORES
    experts_all = chips * CORES
    lines = experts_all + -experts_all % 8
    hidden = w_gate.shape[2]
    out_width = width // 2
    last = chips - 1
    aggregates = max(last - 2, 1)
    lanes = rows + -rows % 128
    spans = 2 * (len(SPANS) - 1)
    anywhere = pl.BlockSpec(memory_space=pl.ANY)
    vmem, dma = pltpu.VMEM, pltpu.SemaphoreType.DMA
    return pl.pallas_call(
        functools.partial(fused_kernel, chips),
        out_shape=vmem((rows, out_width), jnp.bfloat16),
        in_specs=[anywhere] * 7,
        out_specs=pl.BlockSpec(memory_space=vmem),
        scratch_shapes=[
            vmem((rows, width), jnp.bfloat16),
            vmem((1, width), jnp.float32),
            vmem((top_count, rows), jnp.int32),
            vmem((top_count, rows), jnp.float32),
            vmem((chips, rows, width), jnp.bfloat16),
            vmem((chips, lines, lanes), jnp.float32),
            vmem((lanes, lines), jnp.float32),
            vmem((CORES, width, hidden), jnp.bfloat16),
            vmem((CORES, width, hidden), jnp.bfloat16),
            vmem((CORES * hidden, width), jnp.bfloat16),
            vmem((rows, CORES * hidden), jnp.bfloat16),
            vmem((rows, width), jnp.float32),
            vmem((chips, rows, out_width), jnp.float32),
            vmem((2, rows, width), jnp.bfloat16),
            vmem((2, rows, width), jnp.bfloat16),
            vmem((chips, rows, out_width), jnp.bfloat16),
            vmem((chips, rows, out_width), jnp.bfloat16),
            vmem((chips, rows, out_width), jnp.bfloat16),
            vmem((2, rows, out_width), jnp.bfloat16),
            vmem((2, aggregates, rows, out_width), jnp.bfloat16),
            vmem((2, rows, out_width), jnp.bfloat16),
            dma((5,)),
            dma((3,)),
            dma((2, 3)),
            dma((chips + 1,)),
            dma((chips,)),
            dma((chips + 1,)),
            dma((chips, len(PIECES) - 1)),
            dma((chips,)),
            dma((chips,)),
            dma((2,)),
            dma((2, spans)),
            dma((chips,)),
            dma((chips, spans)),
            dma((chips,)),
            dma((2, spans)),
            dma((2, aggregates, spans)),
            dma((2,)),
            dma((2, 2 * OVER)),
        ],
        compiler_params=pltpu.CompilerParams(collective_id=0, has_side_effects=True),
    )(tokens, norm_gain[None, :], expert_ids.T, gate_weights.T, w_gate, w_up, w_down)


def step(mesh, *arrays):
    tokens, norm_gain, w_gate, w_up, w_down, expert_ids, gate_weights = arrays
    ep_count, tp_count = mesh.shape["ep"], mesh.shape["tp"]
    rows, top_count = expert_ids.shape
    experts_all = ep_count * w_gate.shape[0]
    capacity = min(rows, rows * top_count * 4 // (3 * experts_all))
    dense = (
        w_gate.shape[0] == 1
        and tp_count == 2
        and ep_count % CORES == 0
        and ep_count > CORES
        and rows <= 2 * capacity
        and rows % (32 * PIECES[-1]) == 0
        and rows % (32 * SPANS[-1]) == 0
    )
    return fused(*arrays) if dense else body(*arrays)


def solution(mesh):
    placed = (
        P(("grp", "ep"), None),
        P(),
        P("ep", None, "tp"),
        P("ep", None, "tp"),
        P("ep", "tp", None),
        P(("grp", "ep"), None),
        P(("grp", "ep"), None),
    )
    return jax.shard_map(
        functools.partial(step, mesh), mesh=mesh, in_specs=placed, out_specs=P(("grp", "ep"), "tp"), check_vma=False
    )
```

time: 70.5 us -> 64.9 us (0.921)
  Pallas kernels: 68.6 us -> 63.9 us
  local copies, waits for them, and re-layouts: 1.77 us -> 0.75 us
    pallas_call x1, Pallas kernels: 68.6 us -> 63.9 us  [fused(): pl.pallas_call(functools.partial(fused_kernel, chips), out_shape=vmem((ro...]
    unnamed x1, local copies, waits for them, and re-layouts: 1.77 us -> 0.75 us
where the time goes in v4:
time: 64.9 us; the launch traced here: 64.7 us
  Pallas kernels  63.9 us (98%)
  local copies, waits for them, and re-layouts  0.75 us (1%)
    pallas_call x1, Pallas kernels, fused(): pl.pallas_call(functools.partial(fused_kernel, chips), out_shape=vmem((ro...  63.9 us

profile of v4, /device:TPU:0, one launch (start us, length us, event | category | flops | bytes accessed | tf_op | source)
XLA Modules:
  0.0 64.7 jit_solution(15582165720420370221)
XLA Ops:
  0.0 63.9 %shard_map.73 = bf16[192,1024]{1,0:T(8,128)(2,1)S(1)} custom-call(bf16[192,2048]{1,0:T(8,128)(2,1)} %tok_hbm.1, f32[1,2048]{1,0:T(1,128)} %bitcast.3, s32[4,192]{1,0:T(4,128)} %bitcast.4, f32[4,192]{1,0:T(4,128)} %bitcast.5, bf16[1,2048,512]{2,1,0:T(8,128)(2,1)} %wg_hbm.1, bf16[1,2048,512]{2,1,0:T(8,128)(2,1)} %wu_hbm.1, bf16[1,512,2048]{2,1,0:T(8,128)(2,1)} %wd_hbm.1), custom_call_target="tpu_custom_call" | custom-call | tf_op jit(solution)/shard_map/pallas_call | solution.py:652
  63.9 0.7 %copy.9 = bf16[192,1024]{1,0:T(8,128)(2,1)} copy(bf16[192,1024]{1,0:T(8,128)(2,1)S(1)} %shard_map.73) | data formatting | bytes 786432

commit v5 on v4

--- a/solution.py
+++ b/solution.py
@@ -63,8 +63,9 @@
 MESH = pl.DeviceIdType.MESH
 CORES = 2
 PIECES = (0, 1, 3, 5, 6)
-SPANS = (0, 1, 3)
+SPANS = (0, 1, 2, 3)
 OVER = 1
+NEAR = 1
 HIDDEN_TILE = 256
 COLUMN_TILE = 512
 
@@ -100,6 +101,7 @@
     far_in,
     agg_in,
     over_in,
+    near_in,
     input_sem,
     weight_sem,
     pair_sem,
@@ -118,6 +120,8 @@
     agg_recv,
     over_send,
     over_recv,
+    near_send,
+    near_recv,
 ):
     ep, tp = lax.axis_index("ep"), lax.axis_index("tp")
     z, core = lax.div(ep, CORES), lax.rem(ep, CORES)
@@ -390,11 +394,35 @@
             device = chip_of(z + 2 * side - 1)
         return remote(far_out.at[block, span], target, far_send.at[block], receiver, device)
 
+    def near_copy(side, block, which, s):
+        span = span_of(which, s)
+        return remote(
+            far_out.at[block, span],
+            near_in.at[1 - side, span],
+            near_send.at[side],
+            near_recv.at[1 - side, which * NEAR + s],
+            chip_of(block),
+        )
+
+    def outward(turn):
+        block, there = at(turn, 1)
+        return there & (block + 1 - 2 * jnp.where(2 * block < last, 1, 0) == z)
+
+    def over_there(turn):
+        return at(turn, 2)[0] == jnp.where(flow(turn)[0] == 1, last, 0)
+
     def sent(ref, sem):
         return remote(ref, ref, sem, side_recv.at[0, 0], peer)
 
     def arrived(ref, sem):
         return remote(ref, ref, side_send.at[0], sem, peer)
+
+    def outer_starts(side, block, which):
+        for s in range(parts):
+            if s < NEAR:
+                side_copy(block, which, s).start()
+            else:
+                merge_copy(side, 1 - side, which, s, block).start()
 
     def job(distance, turn, which, pumped):
         block, there = at(turn, distance)
@@ -420,9 +448,18 @@
                     merge_out[side, rows_here, begin : begin + COLUMN_TILE] = project(
                         begin, half
                     ).astype(jnp.bfloat16)
-                if turn == 0 or which is second_half:
+                if turn == 0:
                     for s in range(parts):
                         merge_copy(side, 1 - side, which, s, block).start()
+                else:
+                    for s in range(NEAR):
+                        span = span_of(which, s)
+                        side_out[block, span] = merge_out[side, span, pl.ds(theirs, out_width)]
+                        part[block, span] = merge_out[side, span, pl.ds(mine, out_width)].astype(
+                            jnp.float32
+                        )
+                    if which is second_half:
+                        outer_starts(side, block, which)
             else:
                 for begin in range(0, out_width, COLUMN_TILE):
                     side_out[block, rows_here, begin : begin + COLUMN_TILE] = project(
@@ -448,14 +485,27 @@
         if pumped:
             pump()
 
-    def merges_at(turn, which):
-        block, there = at(turn, 1)
-        side = flow(turn)[0]
+    def outer_at(which):
+        block, there = at(1, 1)
+        side = flow(1)[0]
 
         @pl.when(there)
         def _():
-            for s in range(parts):
-                merge_copy(side, 1 - side, which, s, block).start()
+            outer_starts(side, block, which)
+
+    def near_sums():
+        block, there = at(1, 1)
+        side = flow(1)[0]
+
+        @pl.when(there)
+        def _():
+            for which in (second_half, first_half):
+                for s in range(NEAR):
+                    span = span_of(which, s)
+                    side_copy(block, which, s).wait_recv()
+                    total = part[block, span] + side_in[block, span].astype(jnp.float32)
+                    far_out[block, span] = total.astype(jnp.bfloat16)
+                    near_copy(side, block, which, s).start()
 
     def sides_at(distance, turn, which, going):
         block, there = at(turn, distance)
@@ -487,34 +537,60 @@
                         far_out[block, span] = total.astype(jnp.bfloat16)
                         far_copy(side, distance, block, which, s).start()
 
+    early = jnp.logical_not(over_there(0) | over_there(1))
+    for turn in range(2):
+        early = early & (outward(turn) | jnp.logical_not(at(turn, 1)[1]))
+
+    def own_send(which, s):
+        span = span_of(which, s)
+        side_out[z, span] = kept[span, pl.ds(theirs, out_width)].astype(jnp.bfloat16)
+        side_copy(z, which, s).start()
+
+    def own_early(which):
+        @pl.when(early)
+        def _():
+            for s in range(NEAR):
+                own_send(which, s)
+
+    def own_span(which, s):
+        span = span_of(which, s)
+        for turn in range(2):
+            merged = at(turn, 1)[1]
+            if s < NEAR:
+                merged = merged & jnp.logical_not(outward(turn))
+
+            @pl.when(merged)
+            def _(turn=turn):
+                side = flow(turn)[0]
+                arrived(
+                    merge_in.at[side, span], merge_recv.at[side, which * parts + s]
+                ).wait_recv()
+                kept[span] = kept[span] + merge_in[side, span].astype(jnp.float32)
+
+            if s < OVER and chips > 2:
+
+                @pl.when(over_there(turn))
+                def _(turn=turn):
+                    side = flow(turn)[0]
+                    arrived(
+                        over_in.at[side, span], over_recv.at[side, which * OVER + s]
+                    ).wait_recv()
+                    here = (span, pl.ds(theirs, out_width))
+                    kept[here] = kept[here] + over_in[side, span].astype(jnp.float32)
+
+        own_send(which, s)
+
     def own_exchange():
         for which in (first_half, second_half):
             for s in range(parts):
-                span = span_of(which, s)
-                for turn in range(2):
-
-                    @pl.when(at(turn, 1)[1])
-                    def _(turn=turn):
-                        side = flow(turn)[0]
-                        arrived(
-                            merge_in.at[side, span], merge_recv.at[side, which * parts + s]
-                        ).wait_recv()
-                        kept[span] = kept[span] + merge_in[side, span].astype(jnp.float32)
-
-                    if s < OVER and chips > 2:
-                        side = flow(turn)[0]
-                        block = at(turn, 2)[0]
-
-                        @pl.when(block == jnp.where(side == 1, last, 0))
-                        def _(side=side):
-                            arrived(
-                                over_in.at[side, span], over_recv.at[side, which * OVER + s]
-                            ).wait_recv()
-                            here = (span, pl.ds(theirs, out_width))
-                            kept[here] = kept[here] + over_in[side, span].astype(jnp.float32)
-
-                side_out[z, span] = kept[span, pl.ds(theirs, out_width)].astype(jnp.bfloat16)
-                side_copy(z, which, s).start()
+                if s < NEAR:
+
+                    @pl.when(jnp.logical_not(early))
+                    def _():
+                        own_span(which, s)
+
+                else:
+                    own_span(which, s)
 
     def finish():
         for which in (second_half, first_half):
@@ -531,6 +607,17 @@
                                 far_in.at[side, span], far_recv.at[side, which * parts + s]
                             ).wait_recv()
                             kept[here] = kept[here] + far_in[side, span].astype(jnp.float32)
+
+                if s < NEAR:
+                    for turn in range(2):
+
+                        @pl.when(outward(turn))
+                        def _(turn=turn):
+                            side = flow(turn)[0]
+                            arrived(
+                                near_in.at[side, span], near_recv.at[side, which * NEAR + s]
+                            ).wait_recv()
+                            kept[here] = kept[here] + near_in[side, span].astype(jnp.float32)
 
                 side_copy(z, which, s).wait_recv()
                 out_ref[span] = (kept[here] + side_in[z, span].astype(jnp.float32)).astype(
@@ -565,12 +652,12 @@
         if distance < last:
             pump_all(distance + 1)
             if distance == 1:
-                merges_at(1, first_half)
+                outer_at(first_half)
             job(distance + 1, 0, first_half, True)
             if distance + 1 < last:
                 sides_at(distance + 1, 0, first_half, True)
-            if 1 < distance:
-                sides_at(distance, 0, first_half, False)
+            if distance + 1 == last:
+                own_early(first_half)
         if distance in outer:
             wait_x(distance, 1)
             job(distance, 1, second_half, False)
@@ -578,8 +665,13 @@
                 for which in (first_half, second_half):
                     for going in (True, False):
                         sides_at(distance, 1, which, going)
+    if last == 1:
+        own_early(first_half)
     for distance in range(last - 1, 1, -1):
-        sides_at(distance, 0, second_half, False)
+        for which in (first_half, second_half):
+            sides_at(distance, 0, which, False)
+    own_early(second_half)
+    near_sums()
     if last > 1:
         far_sums(last, False)
     own_exchange()
@@ -607,7 +699,13 @@
         @pl.when(at(turn, 1)[1])
         def _(turn=turn):
             side = flow(turn)[0]
-            sent(merge_out.at[side], merge_send.at[side]).wait_send()
+            near_rows = 2 * SPANS[NEAR] * unit if turn == 1 else 0
+            whole = merge_out.at[side, pl.ds(0, rows - near_rows)]
+            sent(whole, merge_send.at[side]).wait_send()
+            if turn == 1:
+                block = at(turn, 1)[0]
+                sent(side_out.at[block, pl.ds(0, near_rows)], side_send.at[block]).wait_send()
+                sent(far_out.at[block, pl.ds(0, near_rows)], near_send.at[side]).wait_send()
 
     finish()
     sent(side_out.at[z], side_send.at[z]).wait_send()
@@ -676,6 +774,7 @@
             vmem((2, rows, out_width), jnp.bfloat16),
             vmem((2, aggregates, rows, out_width), jnp.bfloat16),
             vmem((2, rows, out_width), jnp.bfloat16),
+            vmem((2, rows, out_width), jnp.bfloat16),
             dma((5,)),
             dma((3,)),
             dma((2, 3)),
@@ -694,6 +793,8 @@
             dma((2, aggregates, spans)),
             dma((2,)),
             dma((2, 2 * OVER)),
+            dma((2,)),
+            dma((2, 2 * NEAR)),
         ],
         compiler_params=pltpu.CompilerParams(collective_id=0, has_side_effects=True),
     )(tokens, norm_gain[None, :], expert_ids.T, gate_weights.T, w_gate, w_up, w_down)

time: 64.9 us -> 63.3 us (0.975)
  Pallas kernels: 63.9 us -> 62.3 us
    pallas_call x1, Pallas kernels: 63.9 us -> 62.3 us  [fused(): pl.pallas_call(functools.partial(fused_kernel, chips), out_shape=vmem((ro...]
where the time goes in v5:
time: 63.3 us; the launch traced here: 63.1 us
  Pallas kernels  62.3 us (98%)
  local copies, waits for them, and re-layouts  0.75 us (1%)
    pallas_call x1, Pallas kernels, fused(): pl.pallas_call(functools.partial(fused_kernel, chips), out_shape=vmem((ro...  62.3 us

profile of v5, /device:TPU:0, one launch (start us, length us, event | category | flops | bytes accessed | tf_op | source)
XLA Modules:
  0.0 63.1 jit_solution(1513331486971030861)
XLA Ops:
  0.0 62.3 %shard_map.73 = bf16[192,1024]{1,0:T(8,128)(2,1)S(1)} custom-call(bf16[192,2048]{1,0:T(8,128)(2,1)} %tok_hbm.1, f32[1,2048]{1,0:T(1,128)} %bitcast.3, s32[4,192]{1,0:T(4,128)} %bitcast.4, f32[4,192]{1,0:T(4,128)} %bitcast.5, bf16[1,2048,512]{2,1,0:T(8,128)(2,1)} %wg_hbm.1, bf16[1,2048,512]{2,1,0:T(8,128)(2,1)} %wu_hbm.1, bf16[1,512,2048]{2,1,0:T(8,128)(2,1)} %wd_hbm.1), custom_call_target="tpu_custom_call" | custom-call | tf_op jit(solution)/shard_map/pallas_call | solution.py:750
  62.4 0.7 %copy.9 = bf16[192,1024]{1,0:T(8,128)(2,1)} copy(bf16[192,1024]{1,0:T(8,128)(2,1)S(1)} %shard_map.73) | data formatting | bytes 786432

commit v6 on v5

--- a/solution.py
+++ b/solution.py
@@ -182,7 +182,7 @@
             target = chip_of(flow(turn)[1])
             pl.semaphore_signal(barrier, inc=1, device_id=target, device_id_type=MESH)
 
-    for load in small + loads:
+    for load in small:
         load.start()
 
     def remote(source, target, send, recv, device):
@@ -210,6 +210,8 @@
 
     for load in small[:4]:
         load.wait()
+    for load in loads:
+        load.start()
     normed(tp)
     line = lax.broadcasted_iota(jnp.int32, (codes.shape[1], rows), 0)
     gate = jnp.zeros(line.shape, jnp.float32)
@@ -516,14 +518,14 @@
             for s in range(OVER if distance == 2 and not going else 0, parts):
                 side_copy(block, which, s).start()
 
-    def far_sums(distance, more):
+    def far_sums(distance, more, halves):
         for turn in range(2):
             block, there = at(turn, distance)
             side, _, through = flow(turn)
 
             @pl.when(there & (through if more else jnp.logical_not(through)))
             def _(block=block, side=side):
-                for which in (second_half, first_half):
+                for which in halves:
                     for s in range(OVER if distance == 2 and not more else 0, parts):
                         span = span_of(which, s)
                         side_copy(block, which, s).wait_recv()
@@ -671,13 +673,17 @@
         for which in (first_half, second_half):
             sides_at(distance, 0, which, False)
     own_early(second_half)
-    near_sums()
+    both = (second_half, first_half)
     if last > 1:
-        far_sums(last, False)
+        far_sums(last, False, both)
     own_exchange()
     for distance in range(last - 1, 1, -1):
-        far_sums(distance, False)
-        far_sums(distance, True)
+        far_sums(distance, False, both)
+        if distance > 2:
+            far_sums(distance, True, both)
+    far_sums(2, True, both[:1])
+    near_sums()
+    far_sums(2, True, both[1:])
 
     for give in gives:
         give.wait_send()

time: 63.3 us -> 63 us (level)
  no operation moved by 1% of the time
where the time goes in v6:
time: 63 us; the launch traced here: 62.9 us
  Pallas kernels  62.1 us (99%)
  local copies, waits for them, and re-layouts  0.75 us (1%)
    pallas_call x1, Pallas kernels, fused(): pl.pallas_call(functools.partial(fused_kernel, chips), out_shape=vmem((ro...  62.1 us

profile of v6, /device:TPU:0, one launch (start us, length us, event | category | flops | bytes accessed | tf_op | source)
XLA Modules:
  0.0 62.9 jit_solution(2417039884135484726)
XLA Ops:
  0.0 62.1 %shard_map.73 = bf16[192,1024]{1,0:T(8,128)(2,1)S(1)} custom-call(bf16[192,2048]{1,0:T(8,128)(2,1)} %tok_hbm.1, f32[1,2048]{1,0:T(1,128)} %bitcast.3, s32[4,192]{1,0:T(4,128)} %bitcast.4, f32[4,192]{1,0:T(4,128)} %bitcast.5, bf16[1,2048,512]{2,1,0:T(8,128)(2,1)} %wg_hbm.1, bf16[1,2048,512]{2,1,0:T(8,128)(2,1)} %wu_hbm.1, bf16[1,512,2048]{2,1,0:T(8,128)(2,1)} %wd_hbm.1), custom_call_target="tpu_custom_call" | custom-call | tf_op jit(solution)/shard_map/pallas_call | solution.py:756
  62.1 0.7 %copy.9 = bf16[192,1024]{1,0:T(8,128)(2,1)} copy(bf16[192,1024]{1,0:T(8,128)(2,1)S(1)} %shard_map.73) | data formatting | bytes 786432

commit v7 on v6

--- a/solution.py
+++ b/solution.py
@@ -539,6 +539,7 @@
                         far_out[block, span] = total.astype(jnp.bfloat16)
                         far_copy(side, distance, block, which, s).start()
 
+    inner = (z > 0) & (z < last)
     early = jnp.logical_not(over_there(0) | over_there(1))
     for turn in range(2):
         early = early & (outward(turn) | jnp.logical_not(at(turn, 1)[1]))
@@ -626,27 +627,28 @@
                     jnp.bfloat16
                 )
 
-    for load in loads[:2]:
-        load.wait()
-    pump()
-    activate(z, 0, rows, 0)
-    for _ in range(count - 2):
-        pump()
-    for give in gives[:2]:
-        give.wait_recv()
-    activate(z, 0, rows, 1)
+    def own_compute(there):
+        @pl.when(there)
+        def _():
+            activate(z, 0, rows, 0)
+            activate(z, 0, rows, 1)
+            for begin in range(0, width, COLUMN_TILE):
+                kept[:, begin : begin + COLUMN_TILE] = project(begin, rows)
+
     pump_all(1)
     outer_x()
-    loads[2].wait()
-    gives[2].wait_recv()
-    for begin in range(0, width, COLUMN_TILE):
-        kept[:, begin : begin + COLUMN_TILE] = project(begin, rows)
+    for load in loads:
+        load.wait()
+    for give in gives:
+        give.wait_recv()
 
     outer = range(1, last // 2 + 1)
     job(1, 0, first_half, True)
     for distance in range(1, chips):
         if distance in outer:
             job(distance, 1, first_half, False)
+        if distance == 2:
+            own_compute(inner)
         wait_x(distance, 0)
         job(distance, 0, second_half, distance < last)
         if 1 < distance < last:
@@ -659,6 +661,7 @@
             if distance + 1 < last:
                 sides_at(distance + 1, 0, first_half, True)
             if distance + 1 == last:
+                own_compute(jnp.logical_not(inner))
                 own_early(first_half)
         if distance in outer:
             wait_x(distance, 1)
@@ -816,7 +819,7 @@
         w_gate.shape[0] == 1
         and tp_count == 2
         and ep_count % CORES == 0
-        and ep_count > CORES
+        and ep_count > 3 * CORES
         and rows <= 2 * capacity
         and rows % (32 * PIECES[-1]) == 0
         and rows % (32 * SPANS[-1]) == 0

time: 63 us -> 62.4 us (level)
    pallas_call x1, Pallas kernels: 62.1 us -> 61.5 us  [fused(): pl.pallas_call(functools.partial(fused_kernel, chips), out_shape=vmem((ro...]
where the time goes in v7:
time: 62.4 us; the launch traced here: 62.2 us
  Pallas kernels  61.5 us (99%)
  local copies, waits for them, and re-layouts  0.75 us (1%)
    pallas_call x1, Pallas kernels, fused(): pl.pallas_call(functools.partial(fused_kernel, chips), out_shape=vmem((ro...  61.5 us

profile of v7, /device:TPU:0, one launch (start us, length us, event | category | flops | bytes accessed | tf_op | source)
XLA Modules:
  0.0 62.2 jit_solution(1833957417064212727)
XLA Ops:
  0.0 61.5 %shard_map.73 = bf16[192,1024]{1,0:T(8,128)(2,1)S(1)} custom-call(bf16[192,2048]{1,0:T(8,128)(2,1)} %tok_hbm.1, f32[1,2048]{1,0:T(1,128)} %bitcast.3, s32[4,192]{1,0:T(4,128)} %bitcast.4, f32[4,192]{1,0:T(4,128)} %bitcast.5, bf16[1,2048,512]{2,1,0:T(8,128)(2,1)} %wg_hbm.1, bf16[1,2048,512]{2,1,0:T(8,128)(2,1)} %wu_hbm.1, bf16[1,512,2048]{2,1,0:T(8,128)(2,1)} %wd_hbm.1), custom_call_target="tpu_custom_call" | custom-call | tf_op jit(solution)/shard_map/pallas_call | solution.py:759
  61.5 0.7 %copy.9 = bf16[192,1024]{1,0:T(8,128)(2,1)} copy(bf16[192,1024]{1,0:T(8,128)(2,1)S(1)} %shard_map.73) | data formatting | bytes 786432

commit v8 on v7

--- a/solution.py
+++ b/solution.py
@@ -259,11 +259,11 @@
 
     def x_copy(block, which, q):
         ref = rows_of(block, which, q)
-        return remote(ref, ref, x_send.at[block], x_recv.at[block], peer)
+        return remote(ref, ref, x_send.at[0], x_recv.at[block], peer)
 
     def x_whole(block, which):
         ref = rows_all.at[block, half_of(which)]
-        return remote(ref, ref, x_send.at[block], x_recv.at[block], peer)
+        return remote(ref, ref, x_send.at[0], x_recv.at[block], peer)
 
     for q in range(count):
         for turn in range(2):
@@ -426,7 +426,7 @@
             else:
                 merge_copy(side, 1 - side, which, s, block).start()
 
-    def job(distance, turn, which, pumped):
+    def job(distance, turn, which, pumped, ready=None):
         block, there = at(turn, distance)
         side, _, through = flow(turn)
         start = pl.multiple_of(which * half, 16)
@@ -439,6 +439,8 @@
         def _():
             activate(block, start, half, 1)
 
+        if ready is not None:
+            ready()
         if pumped:
             pump()
 
@@ -637,13 +639,16 @@
 
     pump_all(1)
     outer_x()
-    for load in loads:
-        load.wait()
-    for give in gives:
-        give.wait_recv()
+    for i in range(2):
+        loads[i].wait()
+        gives[i].wait_recv()
 
     outer = range(1, last // 2 + 1)
-    job(1, 0, first_half, True)
+    def down_ready():
+        loads[2].wait()
+        gives[2].wait_recv()
+
+    job(1, 0, first_half, True, down_ready)
     for distance in range(1, chips):
         if distance in outer:
             job(distance, 1, first_half, False)
@@ -690,6 +695,8 @@
 
     for give in gives:
         give.wait_send()
+    gone = rows_all.at[pl.ds(0, last), half_of(tp)]
+    remote(gone, gone, x_send.at[0], x_recv.at[0], peer).wait_send()
     for turn in range(2):
         for distance in range(chips):
             if distance < last:
@@ -698,12 +705,6 @@
                 def _(turn=turn, distance=distance):
                     z_sent(turn, distance).wait_send()
                     code_copy(turn, distance).wait_send()
-
-            if distance > 0:
-
-                @pl.when(at(turn, distance)[1])
-                def _(turn=turn, distance=distance):
-                    x_whole(at(turn, distance)[0], tp).wait_send()
 
         @pl.when(at(turn, 1)[1])
         def _(turn=turn):
@@ -791,7 +792,7 @@
             dma((chips,)),
             dma((chips + 1,)),
             dma((chips, len(PIECES) - 1)),
-            dma((chips,)),
+            dma((1,)),
             dma((chips,)),
             dma((2,)),
             dma((2, spans)),

time: 62.4 us -> 62.4 us (level)
  no operation moved by 1% of the time
where the time goes in v8:
time: 62.4 us; the launch traced here: 62.2 us
  Pallas kernels  61.4 us (98%)
  local copies, waits for them, and re-layouts  0.75 us (1%)
    pallas_call x1, Pallas kernels, fused(): pl.pallas_call(functools.partial(fused_kernel, chips), out_shape=vmem((ro...  61.4 us

profile of v8, /device:TPU:0, one launch (start us, length us, event | category | flops | bytes accessed | tf_op | source)
XLA Modules:
  0.0 62.2 jit_solution(7714963777826527849)
XLA Ops:
  0.0 61.4 %shard_map.73 = bf16[192,1024]{1,0:T(8,128)(2,1)S(1)} custom-call(bf16[192,2048]{1,0:T(8,128)(2,1)} %tok_hbm.1, f32[1,2048]{1,0:T(1,128)} %bitcast.3, s32[4,192]{1,0:T(4,128)} %bitcast.4, f32[4,192]{1,0:T(4,128)} %bitcast.5, bf16[1,2048,512]{2,1,0:T(8,128)(2,1)} %wg_hbm.1, bf16[1,2048,512]{2,1,0:T(8,128)(2,1)} %wu_hbm.1, bf16[1,512,2048]{2,1,0:T(8,128)(2,1)} %wd_hbm.1), custom_call_target="tpu_custom_call" | custom-call | tf_op jit(solution)/shard_map/pallas_call | solution.py:760
  61.4 0.7 %copy.9 = bf16[192,1024]{1,0:T(8,128)(2,1)} copy(bf16[192,1024]{1,0:T(8,128)(2,1)S(1)} %shard_map.73) | data formatting | bytes 786432
